TPU v7x, 512 devices: a whole 4x8x8 slice. The times are simulated.
512 devices in a mesh: sp: 128 (over z, y, core), tp: 4 (over x).
Axes of the slice: x: 4, y: 8, z: 8, core: 2. Of those that a mesh axis runs over, the one named last changes fastest.
Arguments:
- tokens: bfloat16 [32768, 2048], P(('sp', 'tp')), may hold values from -6 to 6
- norm_gain: float32 [2048], replicated, may hold values from 0.1 to 1.9
- query_weight: bfloat16 [1024, 2048], P('tp', 'sp'), may hold values from -0.088609319 to 0.088609319
- key_weight: bfloat16 [256, 2048], P('tp', 'sp'), may hold values from -0.10628699 to 0.10628699
- value_weight: bfloat16 [256, 2048], P('tp', 'sp'), may hold values from -0.125 to 0.125
- gate_weight: bfloat16 [1024, 2048], P('tp', 'sp'), may hold values from -0.125 to 0.125
- left_weight: bfloat16 [1024, 2048], P('tp', 'sp'), may hold values from -0.125 to 0.125
- input_weight: bfloat16 [1024, 2048], P('tp', 'sp'), may hold values from -0.125 to 0.125
- query_gain: float32 [64], replicated, may hold values from 0.3 to 4.5, as said below
- key_gain: float32 [64], replicated, may hold values from 0.3 to 4.5, as said below
- sink_logit: float32 [16], P('tp'), may hold values from 2 to 7
- conv_weight: float32 [3, 1024], P(None, 'tp'), may hold values from -3 to 3
- out_attention: bfloat16 [1024, 2048], P('tp', 'sp'), may hold values from -0.125 to 0.125
- out_conv: bfloat16 [1024, 2048], P('tp', 'sp'), may hold values from -0.125 to 0.125
Outputs:
- mixed: bfloat16 [32768, 2048], P(('sp', 'tp'))
Inputs may be any that keep to these rules, and one draw needn't show every extreme that they name: `query_gain`: positive. `key_gain`: positive.
All inputs are finite; a program needn't handle non-finite values.
Results may differ from a plain program's by a relative error of at most 0.024.
Values may be sent and summed in bfloat16 or wider, within the bound.
No kernel may reach another device: no remote copies, remote signals or barrier semaphores. Data moves between devices by JAX's collectives and lax.ppermute only.
A program may use at most 64 MiB of HBM per device.

v0:
```python
import jax
import jax.numpy as jnp
from jax import lax
from jax.sharding import PartitionSpec as P

HEAD_DIM = 64
WINDOW = 128
BLOCK = 128


EPS = 1e-06
ROPE_BASE = 10000.0
NEG_FILL = -1e30


def turned_gather(arrays, axis, dims):
    turned = [jnp.moveaxis(a, dim, 0) for a, dim in zip(arrays, dims)]
    widths = [t[0].size for t in turned]
    both = jnp.concatenate([t.reshape(-1, w) for t, w in zip(turned, widths)], axis=1)
    out = lax.all_gather(both, axis, axis=0, tiled=True)
    blocks = jnp.split(out, [sum(widths[:k]) for k in range(1, len(widths))], axis=1)
    return tuple(
        (
            jnp.moveaxis(b.reshape(-1, *t.shape[1:]), 0, dim)
            for b, t, dim in zip(blocks, turned, dims)
        )
    )


def from_everyone(value, axis):
    devices = lax.axis_size(axis)
    return lax.all_to_all(
        jnp.broadcast_to(value[None], (devices, *value.shape)), axis, 0, 0, tiled=True
    )


def laid_out(blocks, dim):
    shape = list(blocks.shape[1:])
    shape[dim] *= blocks.shape[0]
    return jnp.moveaxis(blocks, 0, dim).reshape(shape)


def gathered_copies(value, axis, dim):
    blocks = from_everyone(value, axis)
    return laid_out(blocks, dim)


def with_halo(cells, sides, width):
    for axis, dim in sides:
        count = lax.axis_size(axis)
        ends = count - 1
        head = lax.slice_in_dim(cells, 0, width, axis=dim)
        tail = lax.slice_in_dim(cells, cells.shape[dim] - width, cells.shape[dim], axis=dim)
        cells = jnp.concatenate(
            [
                lax.ppermute(tail, axis, [(i, (i + 1) % count) for i in range(ends)]),
                cells,
                lax.ppermute(head, axis, [((i + 1) % count, i) for i in range(ends)]),
            ],
            axis=dim,
        )
    return cells


def split_up(value, dim, devices):
    before, after = (value.shape[:dim], value.shape[dim + 1 :])
    return jnp.moveaxis(value.reshape(*before, devices, -1, *after), dim, 0)


def summed_on_arrival(value, axis, dim):
    blocks = split_up(value, dim, lax.axis_size(axis))
    arrived = lax.all_to_all(blocks, axis, split_axis=0, concat_axis=0, tiled=True)
    return arrived.astype(jnp.float32).sum(axis=0)


def normalize(values, gain):
    return values * lax.rsqrt(jnp.mean(values * values, axis=-1, keepdims=True) + EPS) * gain


def rotate(values, positions):
    half = values.shape[-1] // 2
    freq = ROPE_BASE ** (-jnp.arange(half, dtype=jnp.float32) / half)
    angle = positions[:, None] * freq
    cosine = jnp.cos(angle)[:, None, :]
    sine = jnp.sin(angle)[:, None, :]
    first = values[..., :half]
    second = values[..., half:]
    return jnp.concatenate(
        [first * cosine - second * sine, second * cosine + first * sine], axis=-1
    )


def project(rows, weight):
    return lax.dot_general(
        rows, weight, (((1,), (1,)), ((), ())), preferred_element_type=jnp.float32
    ).astype(jnp.bfloat16)


def attend(query_rot, key_rim, value_rim, sinks, offset, total):
    count = query_rot.shape[0]
    local_heads = query_rot.shape[1]
    kv_local = key_rim.shape[1]
    group = local_heads // kv_local
    span = BLOCK + 2 * WINDOW
    nblocks = count // BLOCK
    shaped = query_rot.reshape(nblocks, BLOCK, kv_local, group, HEAD_DIM)
    sink_group = sinks.reshape(kv_local, group)[:, :, None]

    def one_block(packed):
        block_index, query_block = packed
        begin = block_index * BLOCK
        key_block = lax.dynamic_slice_in_dim(key_rim, begin, span, 0)
        value_block = lax.dynamic_slice_in_dim(value_rim, begin, span, 0)
        scores = jnp.einsum(
            "qkgd,nkd->kgqn", query_block, key_block, preferred_element_type=jnp.float32
        ) * HEAD_DIM ** (-0.5)
        query_pos = offset + begin + jnp.arange(BLOCK, dtype=jnp.int32)
        key_pos = offset + begin - WINDOW + jnp.arange(span, dtype=jnp.int32)
        allowed = (
            (jnp.abs(query_pos[:, None] - key_pos[None, :]) <= WINDOW)
            & (key_pos >= 0)[None, :]
            & (key_pos < total)[None, :]
        )
        scores = jnp.where(allowed, scores, NEG_FILL)
        top = jnp.maximum(jnp.max(scores, axis=-1), sink_group)
        expo = jnp.exp(scores - top[..., None])
        denom = jnp.sum(expo, axis=-1) + jnp.exp(sink_group - top)
        weights = (expo / denom[..., None]).astype(jnp.bfloat16)
        return jnp.einsum(
            "kgqn,nkd->qkgd", weights, value_block, preferred_element_type=jnp.float32
        ).astype(jnp.bfloat16)

    result = lax.map(one_block, (jnp.arange(nblocks, dtype=jnp.int32), shaped))
    return result.reshape(count, local_heads * HEAD_DIM)


def per_device(
    tokens,
    norm_gain,
    query_weight,
    key_weight,
    value_weight,
    gate_weight,
    left_weight,
    input_weight,
    query_gain,
    key_gain,
    sink_logit,
    conv_weight,
    out_attention,
    out_conv,
):
    sp_count = lax.axis_size("sp")
    sp_place = lax.axis_index("sp")
    gathered = turned_gather(
        (
            query_weight,
            key_weight,
            value_weight,
            gate_weight,
            left_weight,
            input_weight,
            out_attention,
            out_conv,
        ),
        "sp",
        (1, 1, 1, 1, 1, 1, 1, 1),
    )
    (
        query_full,
        key_full,
        value_full,
        gate_full,
        left_full,
        input_full,
        attn_out_full,
        conv_out_full,
    ) = gathered
    normed = normalize(tokens.astype(jnp.float32), norm_gain).astype(jnp.bfloat16)
    widths = [
        query_full.shape[0],
        key_full.shape[0],
        value_full.shape[0],
        gate_full.shape[0],
        left_full.shape[0],
        input_full.shape[0],
    ]
    piece = gathered_copies(normed, "tp", 0)
    joined = jnp.concatenate(
        [
            project(piece, weight)
            for weight in (query_full, key_full, value_full, gate_full, left_full, input_full)
        ],
        axis=1,
    )
    count = joined.shape[0]
    bounds = [0]
    for width in widths:
        bounds.append(bounds[-1] + width)
    query, keys, values, gate, left, inputs = [
        joined[:, bounds[place] : bounds[place + 1]] for place in range(6)
    ]
    offset = sp_place * count
    total = count * sp_count
    positions = (offset + jnp.arange(count, dtype=jnp.int32)).astype(jnp.float32)
    local_heads = widths[0] // HEAD_DIM
    kv_local = widths[1] // HEAD_DIM
    query_rot = rotate(
        normalize(query.reshape(count, local_heads, HEAD_DIM).astype(jnp.float32), query_gain),
        positions,
    ).astype(jnp.bfloat16)
    key_rot = rotate(
        normalize(keys.reshape(count, kv_local, HEAD_DIM).astype(jnp.float32), key_gain), positions
    ).astype(jnp.bfloat16)
    key_flat = key_rot.reshape(count, kv_local * HEAD_DIM)
    product = (left.astype(jnp.float32) * inputs.astype(jnp.float32)).astype(jnp.bfloat16)
    kv_width = widths[1]
    joint = with_halo(jnp.concatenate([key_flat, values, product], axis=1), (("sp", 0),), WINDOW)
    pair_rim = joint[:, : 2 * kv_width]
    product_rim = joint[WINDOW - 1 : WINDOW + count + 1, 2 * kv_width :]
    rim_rows = pair_rim.shape[0]
    key_rim = pair_rim[:, :kv_width].reshape(rim_rows, kv_local, HEAD_DIM)
    value_rim = pair_rim[:, kv_width:].reshape(rim_rows, kv_local, HEAD_DIM)
    attended = attend(query_rot, key_rim, value_rim, sink_logit, offset, total)
    padded = product_rim.astype(jnp.float32)
    convolved = (
        conv_weight[0] * padded[:-2] + conv_weight[1] * padded[1:-1] + conv_weight[2] * padded[2:]
    )
    gated = (gate.astype(jnp.float32) * convolved).astype(jnp.bfloat16)
    summed = summed_on_arrival(
        (
            jnp.dot(attended, attn_out_full, preferred_element_type=jnp.float32)
            + jnp.dot(gated, conv_out_full, preferred_element_type=jnp.float32)
        ).astype(jnp.bfloat16),
        "tp",
        0,
    )
    return summed.astype(jnp.bfloat16)


def solution(mesh):
    in_specs = (
        P(("sp", "tp"), None),
        P(),
        P("tp", "sp"),
        P("tp", "sp"),
        P("tp", "sp"),
        P("tp", "sp"),
        P("tp", "sp"),
        P("tp", "sp"),
        P(),
        P(),
        P("tp"),
        P(None, "tp"),
        P("tp", "sp"),
        P("tp", "sp"),
    )
    out_specs = P(("sp", "tp"), None)
    return jax.shard_map(
        per_device, mesh=mesh, in_specs=in_specs, out_specs=out_specs, check_vma=False
    )
```

profile of v0, /device:TPU:17, one launch (start us, length us, event | category | flops | bytes accessed | tf_op | source)
XLA Modules:
  0.0 158.2 jit_solution(5246746027581701336)
XLA Ops:
  6.5 1.5 concatenate.34
  8.1 1.1 fusion.35
  9.2 1.1 fusion.37
  10.3 1.1 broadcast_in_dim.23
  11.4 4.0 %all-to-all-start = ((bf16[4,64,2048]{2,1,0:T(8,128)(2,1)}), bf16[4,64,2048]{2,1,0:T(8,128)(2,1)S(1)}, u32[]{:S(2)}, u32[]{:S(2)}) async-start(bf16[4,64,2048]{2,1,0:T(8,128)(2,1)} %broadcast_in_dim.23), calls=%async_computation | async-start | bytes 2097152 | tf_op jit(solution)/shard_map/all_to_all | solution.py:32
  15.4 0.8 fusion.64
  16.4 13.2 %all-to-all-done = bf16[4,64,2048]{2,1,0:T(8,128)(2,1)S(1)} async-done(((bf16[4,64,2048]{2,1,0:T(8,128)(2,1)}), bf16[4,64,2048]{2,1,0:T(8,128)(2,1)S(1)}, u32[]{:S(2)}, u32[]{:S(2)}) %all-to-all-start) | async-done | bytes 1048608 | tf_op jit(solution)/shard_map/all_to_all | solution.py:32
  29.6 72.0 %all-gather.2.cloned.1.call-done = bf16[2048,1664]{1,0:T(8,128)(2,1)} async-done(((bf16[16,1664]{1,0:T(8,128)(2,1)}), bf16[2048,1664]{1,0:T(8,128)(2,1)}) %all-gather.2.cloned.1.call-update) | async-done | bytes 6815760 | tf_op jit(solution)/shard_map/all_gather | solution.py:20
  101.6 1.5 multiply_reduce_fusion
  103.2 0.7 multiply_bitcast_fusion
  104.1 1.8 %fusion.40 = (f32[256,4]{0,1:T(4,128)S(1)}, bf16[256,256]{0,1:T(8,128)(2,1)S(1)}) fusion(bf16[256,2048]{1,0:T(8,128)(2,1)S(1)} %bitcast.94, bf16[2048,1664]{1,0:T(8,128)(2,1)} %all-gather.2.cloned.1.call-done), kind=kOutput, calls=%fused_computation.59 | convolution fusion | flops 268696576 | bytes 2232320 | tf_op jit(solution)/shard_map/dot_general | solution.py:94
  106.1 1.7 %convolution_convert_fusion.5 = bf16[256,64]{0,1:T(8,128)(2,1)S(1)} fusion(bf16[256,2048]{1,0:T(8,128)(2,1)S(1)} %bitcast.95, bf16[2048,1664]{1,0:T(8,128)(2,1)} %all-gather.2.cloned.1.call-done), kind=kOutput, calls=%fused_computation.40 | convolution fusion | flops 67125248 | bytes 1605632 | tf_op jit(solution)/shard_map/dot_general | solution.py:94
  107.8 1.7 %fusion.25 = f32[256,256]{0,1:T(8,128)S(1)} fusion(bf16[256,2048]{1,0:T(8,128)(2,1)S(1)} %bitcast.96, bf16[2048,1664]{1,0:T(8,128)(2,1)} %all-gather.2.cloned.1.call-done), kind=kOutput, calls=%fused_computation.39 | convolution fusion | flops 268566528 | bytes 2359296 | tf_op jit(solution)/shard_map/dot_general | solution.py:94
  109.5 1.8 %fusion.24 = bf16[256,256]{0,1:T(8,128)(2,1)S(1)} fusion(f32[256,256]{0,1:T(8,128)S(1)} %fusion.25, bf16[256,2048]{1,0:T(8,128)(2,1)S(1)} %bitcast.97, bf16[2048,1664]{1,0:T(8,128)(2,1)} %all-gather.2.cloned.1.call-done), kind=kOutput, calls=%fused_computation.37 | convolution fusion | flops 268697600 | bytes 2490368 | tf_op jit(solution)/shard_map/dot_general | solution.py:94
  111.3 3.0 %collective-permute-start = (bf16[128,384]{0,1:T(8,128)(2,1)S(1)}, bf16[128,384]{0,1:T(8,128)(2,1)S(1)}, u32[]{:S(2)}, u32[]{:S(2)}) collective-permute-start(bf16[128,384]{0,1:T(8,128)(2,1)S(1)} %get-tuple-element.139), channel_id=1, source_target_pairs={{0,4},{4,8},{8,12},{12,16},{16,20},{20,24},{24,28},{28,32},{32,36}... | collective-permute-start | bytes 294920 | tf_op jit(solution)/shard_map/ppermute | solution.py:56
  114.3 1.9 %collective-permute-start.1 = (bf16[128,384]{0,1:T(8,128)(2,1)S(1)}, bf16[128,384]{0,1:T(8,128)(2,1)S(1)}, u32[]{:S(2)}, u32[]{:S(2)}) collective-permute-start(bf16[128,384]{0,1:T(8,128)(2,1)S(1)} %get-tuple-element.140), channel_id=1, source_target_pairs={{4,0},{8,4},{12,8},{16,12},{20,16},{24,20},{28,24},{32,28},{36,32}... | collective-permute-start | bytes 294920 | tf_op jit(solution)/shard_map/ppermute | solution.py:58
  116.5 3.8 %collective-permute-done.1 = bf16[128,384]{0,1:T(8,128)(2,1)S(1)} collective-permute-done((bf16[128,384]{0,1:T(8,128)(2,1)S(1)}, bf16[128,384]{0,1:T(8,128)(2,1)S(1)}, u32[]{:S(2)}, u32[]{:S(2)}) %collective-permute-start.1) | collective-permute-done | bytes 98336 | tf_op jit(solution)/shard_map/ppermute | solution.py:58
  120.3 4.8 %while.12 = (s32[]{:T(128)}, bf16[2,128,1,4,64]{1,4,3,2,0:T(8,128)(2,1)S(1)}, s32[2]{0:T(128)S(1)}, bf16[512,1,64]{0,2,1:T(8,128)(2,1)S(1)}, s32[]{:T(128)}, /*i...) while((s32[]{:T(128)}, ...), condition=%wide.region_6.7_spmd, body=%wide.region_3.6_spmd.sunk | while | flops 52185736 | bytes 2713363 | solution.py:133
  120.3 0.6 dynamic_slice.49
  122.7 0.6 dynamic_slice.49
  125.5 1.7 %fusion.30 = f32[256,2048]{1,0:T(8,128)S(1)} fusion(bf16[2048,1664]{1,0:T(8,128)(2,1)} %all-gather.2.cloned.1.call-done, bf16[32,8,2,128]{3,2,1,0:T(2,128)(2,1)S(1)} %bitcast.100), kind=kOutput, calls=%fused_computation.45 | convolution fusion | flops 268435456 | bytes 3276800 | tf_op jit(solution)/shard_map/dot_general | solution.py:232
  127.2 3.9 %fusion.18 = bf16[256,2048]{1,0:T(8,128)(2,1)} fusion(f32[256,2048]{1,0:T(8,128)S(1)} %fusion.30, bf16[256,2048]{1,0:T(8,128)(2,1)S(1)} %bitcast.98, bf16[2048,1664]{1,0:T(8,128)(2,1)} %all-gather.2.cloned.1.call-done, f32[258,256]{0,1:T(8,128)S(1)} %fusion.46, f32[256]{0:T(256)S(1)} %bitcast.113, f32[256]{0:T(256)S(1)} %bitcast.114, f32[256]{0:T(256)S(1)} %bitcast.112), kind=kOutput, calls=%fused_computation.28 | convolution fusion | flops 538509312 | bytes 7080960 | tf_op jit(solution)/shard_map/dot_general | solution.py:233
  131.1 19.3 %all_to_all.10 = bf16[4,64,2048]{2,1,0:T(8,128)(2,1)S(1)} all-to-all(bf16[4,64,2048]{2,1,0:T(8,128)(2,1)} %bitcast.99), channel_id=1, replica_groups=mesh['sp'=128,'tp'=4] {'tp'}, dimensions={0} | all-to-all | bytes 2097152 | tf_op jit(solution)/shard_map/all_to_all | solution.py:72
  150.4 0.9 reduce_sum.51
  (45 shorter events, 3.4 us)
Async XLA Ops:
  6.5 99.4 %copy-start.1 = (f32[64]{0:T(128)S(1)}, f32[64]{0:T(128)}, u32[]{:S(2)}) copy-start(f32[64]{0:T(128)} %param.24) | copy-start | bytes 772
  6.5 95.1 %all-gather.2.cloned.1.call-start = ((), (), s32[]{:S(2)}) async-start(), calls=%async_computation.2 | async-start | bytes 6868992 | tf_op jit(solution)/shard_map/all_gather | solution.py:20
  11.4 18.3 %all-to-all-start = ((bf16[4,64,2048]{2,1,0:T(8,128)(2,1)}), bf16[4,64,2048]{2,1,0:T(8,128)(2,1)S(1)}, u32[]{:S(2)}, u32[]{:S(2)}) async-start(bf16[4,64,2048]{2,1,0:T(8,128)(2,1)} %broadcast_in_dim.23), calls=%async_computation | async-start | bytes 2097152 | tf_op jit(solution)/shard_map/all_to_all | solution.py:32
  101.6 18.7 %copy-start = (f32[4]{0:T(128)S(1)}, f32[4]{0:T(128)}, u32[]{:S(2)}) copy-start(f32[4]{0:T(128)} %param.26) | copy-start | bytes 52
  111.3 5.2 %collective-permute-start = (bf16[128,384]{0,1:T(8,128)(2,1)S(1)}, bf16[128,384]{0,1:T(8,128)(2,1)S(1)}, u32[]{:S(2)}, u32[]{:S(2)}) collective-permute-start(bf16[128,384]{0,1:T(8,128)(2,1)S(1)} %get-tuple-element.139), channel_id=1, source_target_pairs={{0,4},{4,8},{8,12},{12,16},{16,20},{20,24},{24,28},{28,32},{32,36}... | collective-permute-start | bytes 294920 | tf_op jit(solution)/shard_map/ppermute | solution.py:56
  114.3 5.9 %collective-permute-start.1 = (bf16[128,384]{0,1:T(8,128)(2,1)S(1)}, bf16[128,384]{0,1:T(8,128)(2,1)S(1)}, u32[]{:S(2)}, u32[]{:S(2)}) collective-permute-start(bf16[128,384]{0,1:T(8,128)(2,1)S(1)} %get-tuple-element.140), channel_id=1, source_target_pairs={{4,0},{8,4},{12,8},{16,12},{20,16},{24,20},{28,24},{32,28},{36,32}... | collective-permute-start | bytes 294920 | tf_op jit(solution)/shard_map/ppermute | solution.py:58
Sparse Core Ops, SparseCore 0:
  10.5 91.0 all-gather.1
where the time goes:
time: 159 us; the launch traced here: 158 us
  waiting for transfers between devices  89 us (56%)
  blocking collectives  19.3 us (12%)
  matrix products  15.3 us (10%)
  between operations  13.6 us (9%)
  starting transfers between devices  8.94 us (6%)
  other arithmetic  5.81 us (4%)
  local copies, waits for them, and re-layouts  4.8 us (3%)
    all_gather x1, waiting for transfers between devices, turned_gather(): out = lax.all_gather(both, axis, axis=0, tiled=True)  72 us
    all_to_all x1, blocking collectives, summed_on_arrival(): lax.all_to_all(blocks, axis, split_axis=0, concat_axis=0, tiled=True)  19.3 us
    all_to_all x1, waiting for transfers between devices, from_everyone(): lax.all_to_all(jnp.broadcast_to(value[None], (devices, *value.shape)), ax...  13.2 us
    dot_general x5, matrix products, project(): lax.dot_general(rows, weight, (((1,), (1,)), ((), ())), preferred_element...  8.46 us
    all_to_all x1, starting transfers between devices, from_everyone(): lax.all_to_all(jnp.broadcast_to(value[None], (devices, *value.shape)), ax...  4.01 us
    dot_general x1, matrix products, per_device(): jnp.dot(gated, conv_out_full, preferred_element_type=jnp.float32)  3.94 us
    ppermute x1, waiting for transfers between devices, with_halo(): lax.ppermute(head, axis, [((i + 1) % count, i) for i in range(ends)])  3.79 us
  transfers between devices with their start and end apart: 4, of which 3 were waited for; matrix products, arithmetic and copies ran while one was open for 3% of the time, Pallas kernels for 0%

commit v1 on v0

v1 whole, which is shorter than its diff:
```python
import jax
import jax.numpy as jnp
import numpy as np
from jax import lax
from jax.experimental import pallas as pl
from jax.experimental.pallas import tpu as pltpu
from jax.sharding import PartitionSpec as P


HEAD = 64
HALF = HEAD // 2
WINDOW = 128
BLOCK = 128
EPS = 1e-06
ROPE_BASE = 10000.0
NEG_FILL = -1e30
RING = 8
TP = 4
CHIPS = RING * RING
LOCAL = 64
CHIP_TOKENS = 2 * TP * LOCAL
ROWS = CHIP_TOKENS + 2 * WINDOW
PROJ = 640
OUTW = 256
WIDTH = PROJ + OUTW


def sp_of(z, y, c):
    return (z * RING + y) * 2 + c


def even_partner(pos):
    return pos ^ 1


def odd_partner(pos):
    return (pos - 1) % RING if pos % 2 == 0 else (pos + 1) % RING


def matching(partner):
    pairs = []
    for z in range(RING):
        for y in range(RING):
            pairs.append((sp_of(z, y, 0), sp_of(z, partner(y), 0)))
            pairs.append((sp_of(z, y, 1), sp_of(partner(z), y, 1)))
    return pairs


EVEN = matching(even_partner)
ODD = matching(odd_partner)
SWAP = [(2 * k + c, 2 * k + 1 - c) for k in range(CHIPS) for c in range(2)]
GROUPS = [[sp_of(z, y, 0) for z in range(RING)] for y in range(RING)] + [
    [sp_of(z, y, 1) for y in range(RING)] for z in range(RING)
]
HALOS = [
    [
        ((2 * k + 1) * TP + x, (2 * k + 2 + c) * TP + x) for k in range(CHIPS - 1) for x in (2, 3)
    ]
    + [((2 * k + 2) * TP + x, (2 * k + c) * TP + x) for k in range(CHIPS - 1) for x in (0, 1)]
    for c in range(2)
]
PART = LOCAL // 2
SHARE = LOCAL + PART
ANGLES = np.tile(ROPE_BASE ** (-np.arange(HALF) / HALF), 128 // HALF).astype(np.float32)
VMEM = pl.BlockSpec(memory_space=pltpu.VMEM)
SMEM = pl.BlockSpec(memory_space=pltpu.SMEM)


def columns_kernel(q, k, v, g, l, i, oa, oc, out):
    at = 0
    for c in range(2):
        for ref in (q, k, v, g, l, i, oa, oc):
            if ref.shape[1] == HEAD:
                width, first = HEAD, 0
            else:
                width, first = 128, c * 128
            out[:, at : at + width] = ref[:, first : first + width]
            at += width


def columns(weights):
    return pl.pallas_call(
        columns_kernel,
        out_shape=jax.ShapeDtypeStruct((weights[0].shape[1], 2 * WIDTH), jnp.bfloat16),
        in_specs=[VMEM] * len(weights),
        out_specs=VMEM,
        name="columns",
    )(*[w.T for w in weights])


def copies_kernel(where_ref, mine_ref, got_ref, out):
    core = where_ref[2]
    for to, ref in enumerate((mine_ref, got_ref)):
        block = jnp.where(core == 0, ref[:, :WIDTH], ref[:, WIDTH:])
        for k in range(RING):
            out[k, to * 16 : (to + 1) * 16, :] = block


def copies(where, mine, got):
    return pl.pallas_call(
        copies_kernel,
        out_shape=jax.ShapeDtypeStruct((RING, 32, WIDTH), jnp.bfloat16),
        in_specs=[SMEM, VMEM, VMEM],
        out_specs=VMEM,
        name="copies",
    )(where, mine, got)


def rows_kernel(normed, rim0, rim1, out):
    rim = rim0[...] + rim1[...]
    for x in range(TP):
        out[x, :LOCAL, :] = normed[...]
        out[x, LOCAL:, :] = rim


def row_copies(normed, rim0, rim1):
    return pl.pallas_call(
        rows_kernel,
        out_shape=jax.ShapeDtypeStruct((TP, SHARE, normed.shape[1]), jnp.bfloat16),
        in_specs=[VMEM] * 3,
        out_specs=VMEM,
        name="rows",
    )(normed, rim0, rim1)


def gathered_weights(where, mine):
    got = lax.ppermute(mine, "sp", SWAP)
    blocks = copies(where, mine, got)
    own = lax.all_to_all(blocks, "sp", 0, 0, axis_index_groups=GROUPS, tiled=True)
    own = own.reshape(RING * 32, WIDTH)
    e1 = lax.ppermute(own, "sp", EVEN)
    o1 = lax.ppermute(own, "sp", ODD)
    o2 = lax.ppermute(e1, "sp", ODD)
    e2 = lax.ppermute(o1, "sp", EVEN)
    e3 = lax.ppermute(o2, "sp", EVEN)
    o3 = lax.ppermute(e2, "sp", ODD)
    o4 = lax.ppermute(e3, "sp", ODD)
    return own, e1, o1, e2, o2, e3, o3, o4


def norm_kernel(x_ref, gain_ref, normed, part0, part1):
    wide = x_ref[...].astype(jnp.float32)
    mean = jnp.mean(wide * wide, axis=-1, keepdims=True)
    value = (wide * lax.rsqrt(mean + EPS) * gain_ref[...]).astype(jnp.bfloat16)
    normed[...] = value
    part0[...] = value[:PART]
    part1[...] = value[PART:]


def normalized(tokens, norm_gain):
    rows, features = tokens.shape
    part = jax.ShapeDtypeStruct((PART, features), jnp.bfloat16)
    return pl.pallas_call(
        norm_kernel,
        out_shape=(jax.ShapeDtypeStruct((rows, features), jnp.bfloat16), part, part),
        in_specs=[VMEM] * 2,
        out_specs=(VMEM,) * 3,
        name="norm",
    )(tokens, norm_gain[None])


def gathered_tokens(normed, part0, part1):
    both = ("sp", "tp")
    rim0 = lax.ppermute(part0, both, HALOS[0])
    rim1 = lax.ppermute(part1, both, HALOS[1])
    sent = row_copies(normed, rim0, rim1)
    mine = lax.all_to_all(sent, "tp", 0, 0, tiled=True).reshape(TP * SHARE, -1)
    return mine, lax.ppermute(mine, "sp", SWAP)


def layer_kernel(
    where_ref,
    sink_ref,
    x_ref,
    x2_ref,
    own,
    e1,
    o1,
    e2,
    o2,
    e3,
    o3,
    o4,
    cos_ref,
    sin_ref,
    qg_ref,
    kg_ref,
    conv_ref,
    kept_ref,
    sent_ref,
    w_s,
    p_s,
    kk_s,
    vv_s,
    prod_s,
    act_s,
):
    pos, sgn, core, chip = where_ref[0], where_ref[1], where_ref[2], where_ref[3]

    def place(piece, steps):
        at = lax.rem(pos + sgn * steps + 2 * RING, RING)
        for j in range(RING):
            start = jnp.where(core == 0, j * 256 + at * 32, at * 256 + j * 32)
            for h in range(2):
                to = start + 16 * (core if h == 0 else 1 - core)
                w_s[pl.ds(pl.multiple_of(to, 16), 16), :] = piece[
                    j * 32 + h * 16 : j * 32 + h * 16 + 16, :
                ]

    place(own, 0)
    place(e1, 1)
    place(o1, -1)
    place(e2, 2)
    place(o2, -2)
    place(e3, 3)
    place(o3, -3)
    place(o4, -4)

    for ref, c in ((x_ref, core), (x2_ref, 1 - core)):
        tokens = ref[...]
        for lo, hi in ((0, 256), (256, 512), (512, PROJ)):
            part = jnp.dot(tokens, w_s[:, lo:hi], preferred_element_type=jnp.float32).astype(
                jnp.bfloat16
            )
            for x in range(TP):
                base = x * SHARE
                to = WINDOW + x * LOCAL + c * (TP * LOCAL)
                p_s[pl.ds(pl.multiple_of(to, LOCAL), LOCAL), lo:hi] = part[base : base + LOCAL]
                to = ((x - 2) * LOCAL if x >= 2 else WINDOW + CHIP_TOKENS + x * LOCAL) + c * PART
                p_s[pl.ds(pl.multiple_of(to, PART), PART), lo:hi] = part[base + LOCAL : base + SHARE]

    def gain_rows(ref, scale):
        gain = jnp.concatenate([ref[...], ref[...]], axis=1) * scale
        lane = lax.rem(lax.broadcasted_iota(jnp.int32, gain.shape, 1), HEAD)
        low = pltpu.roll(gain, 128 - HALF, 1)
        return gain, jnp.where(lane < HALF, -low, pltpu.roll(gain, HALF, 1))

    query_gain = gain_rows(qg_ref, HEAD ** (-0.5))
    key_gain = gain_rows(kg_ref, 1.0)

    def rotated(value, at, gain, crossed_gain):
        lane = lax.broadcasted_iota(jnp.int32, value.shape, 1)
        low = lane < HEAD
        square = value * value
        mean0 = jnp.sum(jnp.where(low, square, 0.0), axis=-1, keepdims=True) * (1.0 / HEAD)
        mean1 = jnp.sum(jnp.where(low, 0.0, square), axis=-1, keepdims=True) * (1.0 / HEAD)
        scaled = value * jnp.where(low, lax.rsqrt(mean0 + EPS), lax.rsqrt(mean1 + EPS))
        crossed = jnp.where(
            lax.rem(lane, HEAD) < HALF,
            pltpu.roll(scaled, 2 * HEAD - HALF, 1),
            pltpu.roll(scaled, HALF, 1),
        )
        cosine = cos_ref[at : at + BLOCK, :]
        sine = sin_ref[at : at + BLOCK, :]
        return scaled * (cosine * gain) + crossed * (sine * crossed_gain)

    for at in range(0, ROWS, BLOCK):
        kv = p_s[at : at + BLOCK, 128:256].astype(jnp.float32)
        lane = lax.broadcasted_iota(jnp.int32, kv.shape, 1)
        key = rotated(kv, at, *key_gain)
        kk_s[at : at + BLOCK, :] = jnp.where(lane < HEAD, key, pltpu.roll(key, HEAD, 1)).astype(
            jnp.bfloat16
        )
        vv_s[at : at + BLOCK, :] = jnp.where(lane < HEAD, pltpu.roll(kv, HEAD, 1), kv).astype(
            jnp.bfloat16
        )
        prod_s[at : at + BLOCK, :] = (
            (
                p_s[at : at + BLOCK, 384:512].astype(jnp.float32)
                * p_s[at : at + BLOCK, 512:640].astype(jnp.float32)
            )
            .astype(jnp.bfloat16)
            .astype(jnp.float32)
        )

    conv = jnp.where(core == 0, conv_ref[:, :128], conv_ref[:, 128:])
    for at in range(0, CHIP_TOKENS, BLOCK):
        rows = slice(at + WINDOW, at + WINDOW + BLOCK)
        query = rotated(p_s[rows, 0:128].astype(jnp.float32), at + WINDOW, *query_gain)
        low = lax.broadcasted_iota(jnp.int32, query.shape, 1) < HEAD
        keys = kk_s[at : at + 3 * BLOCK, :]
        values = vv_s[at : at + 3 * BLOCK, :]
        shape = (BLOCK, 3 * BLOCK)
        q_at = lax.broadcasted_iota(jnp.int32, shape, 0)
        k_at = lax.broadcasted_iota(jnp.int32, shape, 1) - WINDOW
        k_pos = k_at + (chip * CHIP_TOKENS + at)
        allowed = (
            (jnp.abs(q_at - k_at) <= WINDOW) & (k_pos >= 0) & (k_pos < CHIPS * CHIP_TOKENS)
        )
        outs = []
        for head in range(2):
            q_head = jnp.where(low if head == 0 else ~low, query, 0.0).astype(jnp.bfloat16)
            scores = lax.dot_general(
                q_head, keys, (((1,), (1,)), ((), ())), preferred_element_type=jnp.float32
            )
            scores = jnp.where(allowed, scores, NEG_FILL)
            sink = sink_ref[2 * core + head]
            top = jnp.maximum(jnp.max(scores, axis=-1, keepdims=True), sink)
            expo = jnp.exp(scores - top)
            total = jnp.sum(expo, axis=-1, keepdims=True) + jnp.exp(sink - top)
            weights = (expo * (1.0 / total)).astype(jnp.bfloat16)
            outs.append(jnp.dot(weights, values, preferred_element_type=jnp.float32))
        act_s[at : at + BLOCK, 0:128] = jnp.where(low, outs[0], outs[1]).astype(jnp.bfloat16)
        lo = at + WINDOW
        mixed = (
            conv[0:1, :] * prod_s[lo - 1 : lo - 1 + BLOCK, :]
            + conv[1:2, :] * prod_s[lo : lo + BLOCK, :]
            + conv[2:3, :] * prod_s[lo + 1 : lo + 1 + BLOCK, :]
        )
        act_s[at : at + BLOCK, 128:256] = (p_s[rows, 256:384].astype(jnp.float32) * mixed).astype(
            jnp.bfloat16
        )

    half = CHIP_TOKENS // 2
    for ref, c in ((sent_ref, 1 - core), (kept_ref, core)):
        for at in range(0, half, BLOCK):
            ref[at : at + BLOCK, :] = lax.dot_general(
                act_s[pl.ds(pl.multiple_of(c * half + at, BLOCK), BLOCK), :],
                w_s[:, PROJ:],
                (((1,), (1,)), ((), ())),
                preferred_element_type=jnp.float32,
            ).astype(jnp.bfloat16)


def run_layer(where, sinks, tokens, pieces, tables, conv):
    features = tokens[0].shape[-1]
    shape = jax.ShapeDtypeStruct((CHIP_TOKENS // 2, features), jnp.bfloat16)
    return pl.pallas_call(
        layer_kernel,
        out_shape=(shape, shape),
        in_specs=[SMEM, SMEM] + [VMEM] * (len(tokens) + len(pieces) + len(tables) + 1),
        out_specs=(VMEM, VMEM),
        scratch_shapes=[
            pltpu.VMEM((features, WIDTH), jnp.bfloat16),
            pltpu.VMEM((ROWS, PROJ), jnp.bfloat16),
            pltpu.VMEM((ROWS, 128), jnp.bfloat16),
            pltpu.VMEM((ROWS, 128), jnp.bfloat16),
            pltpu.VMEM((ROWS, 128), jnp.float32),
            pltpu.VMEM((CHIP_TOKENS, 256), jnp.bfloat16),
        ],
        compiler_params=pltpu.CompilerParams(vmem_limit_bytes=48 * 1024 * 1024),
        name="layer",
    )(where, sinks, *tokens, *pieces, *tables, conv)


def per_device(
    tokens,
    norm_gain,
    query_weight,
    key_weight,
    value_weight,
    gate_weight,
    left_weight,
    input_weight,
    query_gain,
    key_gain,
    sink_logit,
    conv_weight,
    out_attention,
    out_conv,
):
    sp_place = lax.axis_index("sp").astype(jnp.int32)
    core = lax.rem(sp_place, 2)
    chip = sp_place // 2
    y = lax.rem(chip, RING)
    z = chip // RING
    pos = jnp.where(core == 0, y, z)
    sgn = 1 - 2 * lax.rem(pos, 2)

    where = jnp.stack([pos, sgn, core, chip])
    mine = columns(
        (
            query_weight,
            key_weight,
            value_weight,
            gate_weight,
            left_weight,
            input_weight,
            out_attention,
            out_conv,
        )
    )
    rows = normalized(tokens, norm_gain)
    gathered = gathered_tokens(*rows)
    pieces = gathered_weights(where, mine)

    positions = (chip * CHIP_TOKENS - WINDOW + jnp.arange(ROWS, dtype=jnp.int32)).astype(
        jnp.float32
    )
    angle = positions[:, None] * ANGLES
    tables = (jnp.cos(angle), jnp.sin(angle), query_gain[None], key_gain[None])
    kept, sent = run_layer(where, sink_logit, gathered, pieces, tables, conv_weight)

    arrived = lax.ppermute(sent, "sp", SWAP)
    group = (kept.astype(jnp.float32) + arrived.astype(jnp.float32)).astype(jnp.bfloat16)
    blocks = lax.all_to_all(group.reshape(TP, LOCAL, -1), "tp", 0, 0, tiled=True)
    return blocks.astype(jnp.float32).sum(axis=0).astype(jnp.bfloat16)


def solution(mesh):
    in_specs = (
        P(("sp", "tp"), None),
        P(),
        P("tp", "sp"),
        P("tp", "sp"),
        P("tp", "sp"),
        P("tp", "sp"),
        P("tp", "sp"),
        P("tp", "sp"),
        P(),
        P(),
        P("tp"),
        P(None, "tp"),
        P("tp", "sp"),
        P("tp", "sp"),
    )
    out_specs = P(("sp", "tp"), None)

    return jax.shard_map(
        per_device, mesh=mesh, in_specs=in_specs, out_specs=out_specs, check_vma=False
    )
```

time: 159 us -> 134 us (0.84)
  the two profiles are of different devices: /device:TPU:17 before, /device:TPU:1 now
where the time goes in v1:
time: 134 us
  starting transfers between devices  53.8 us (40%)
  waiting for transfers between devices  40.1 us (30%)
  Pallas kernels  17.7 us (13%)
  blocking collectives  17.2 us (13%)
  other arithmetic  3.34 us (2%)
    all_to_all x1, blocking collectives, per_device(): lax.all_to_all(group.reshape(TP, LOCAL, -1), 'tp', 0, 0, tiled=True)  17.2 us
    all_to_all x1, waiting for transfers between devices, gathered_tokens(): mine = lax.all_to_all(sent, 'tp', 0, 0, tiled=True).reshape(TP * SHARE, -1)  14.6 us
    pallas_call x1, Pallas kernels, run_layer(): pl.pallas_call(layer_kernel, out_shape=(shape, shape), in_specs=[SMEM, SM...  10.3 us
    ppermute x1, starting transfers between devices, gathered_weights(): got = lax.ppermute(mine, 'sp', SWAP)  8.73 us
    ppermute x1, starting transfers between devices, gathered_weights(): o1 = lax.ppermute(own, 'sp', ODD)  7.95 us
    ppermute x1, waiting for transfers between devices, gathered_tokens(): rim1 = lax.ppermute(part1, both, HALOS[1])  7.63 us
    ppermute x1, starting transfers between devices, gathered_weights(): e1 = lax.ppermute(own, 'sp', EVEN)  6.22 us
    all_to_all x1, starting transfers between devices, gathered_tokens(): mine = lax.all_to_all(sent, 'tp', 0, 0, tiled=True).reshape(TP * SHARE, -1)  4.92 us
  transfers between devices with their start and end apart: 14, of which 9 were waited for; matrix products, arithmetic and copies ran while one was open for 2% of the time, Pallas kernels for 3%

profile of v1, /device:TPU:1, one launch (start us, length us, event | category | flops | bytes accessed | tf_op | source)
XLA Modules:
  0.0 133.7 jit_solution(16066549433302519426)
XLA Ops:
  1.5 8.7 %collective-permute-start.3 = (bf16[16,1792]{1,0:T(8,128)(2,1)}, bf16[16,1792]{1,0:T(8,128)(2,1)S(1)}, u32[]{:S(2)}, u32[]{:S(2)}) collective-permute-start(bf16[16,1792]{1,0:T(8,128)(2,1)} %columns.1.mine_ref), channel_id=1, source_target_pairs={{0,4},{4,0},{8,12},{12,8},{16,20},{20,16},{24,28},{28,24},{32,36},... | collective-permute-start | bytes 172040 | tf_op jit(solution)/shard_map/ppermute | solution.py:127
  12.0 1.7 %copies.1 = bf16[8,32,896]{2,1,0:T(8,128)(2,1)} custom-call(s32[4]{0:T(128)} %pad_add_fusion.where_ref, bf16[16,1792]{1,0:T(8,128)(2,1)} %columns.1.mine_ref, bf16[16,1792]{1,0:T(8,128)(2,1)} %copy-done.7), custom_call_target="tpu_custom_call" | custom-call | tf_op jit(solution)/shard_map/copies/pallas_call | solution.py:100
  13.6 3.5 %all-to-all-start.1 = ((bf16[8,32,896]{2,1,0:T(8,128)(2,1)}), bf16[8,32,896]{2,1,0:T(8,128)(2,1)S(1)}, u32[]{:S(2)}, u32[]{:S(2)}) async-start(bf16[8,32,896]{2,1,0:T(8,128)(2,1)} %copies.1), calls=%async_computation.1 | async-start | bytes 917504 | tf_op jit(solution)/shard_map/all_to_all | solution.py:129
  17.1 1.9 %norm.1 = (bf16[64,2048]{1,0:T(8,128)(2,1)}, bf16[32,2048]{1,0:T(8,128)(2,1)}, bf16[32,2048]{1,0:T(8,128)(2,1)}) custom-call(bf16[64,2048]{1,0:T(8,128)(2,1)} %x_ref.1, f32[1,2048]{1,0:T(1,128)} %bitcast.30), custom_call_target="tpu_custom_call" | custom-call | tf_op jit(solution)/shard_map/norm/pallas_call | solution.py:153
  21.0 7.6 %collective-permute-done.1.rim1 = bf16[32,2048]{1,0:T(8,128)(2,1)S(1)} collective-permute-done((bf16[32,2048]{1,0:T(8,128)(2,1)}, bf16[32,2048]{1,0:T(8,128)(2,1)S(1)}, u32[]{:S(2)}, u32[]{:S(2)}) %collective-permute-start.1) | collective-permute-done | bytes 131104 | tf_op jit(solution)/shard_map/ppermute | solution.py:165
  29.2 2.3 %rows.1 = bf16[4,96,2048]{2,1,0:T(8,128)(2,1)} custom-call(bf16[64,2048]{1,0:T(8,128)(2,1)} %get-tuple-element.10.normed, bf16[32,2048]{1,0:T(8,128)(2,1)} %copy-done.5, bf16[32,2048]{1,0:T(8,128)(2,1)} %copy-done.6), custom_call_target="tpu_custom_call" | custom-call | tf_op jit(solution)/shard_map/rows/pallas_call | solution.py:117
  31.6 4.9 %all-to-all-start = ((bf16[4,96,2048]{2,1,0:T(8,128)(2,1)}), bf16[4,96,2048]{2,1,0:T(8,128)(2,1)}, u32[]{:S(2)}, u32[]{:S(2)}) async-start(bf16[4,96,2048]{2,1,0:T(8,128)(2,1)} %rows.1), calls=%async_computation | async-start | bytes 3145728 | tf_op jit(solution)/shard_map/all_to_all | solution.py:167
  36.5 6.2 %collective-permute-start.4 = (bf16[256,896]{1,0:T(8,128)(2,1)S(1)}, bf16[256,896]{1,0:T(8,128)(2,1)S(1)}, u32[]{:S(2)}, u32[]{:S(2)}) collective-permute-start(bf16[256,896]{1,0:T(8,128)(2,1)S(1)} %bitcast.18), channel_id=1, source_target_pairs={{0,8},{4,68},{8,0},{12,76},{16,24},{20,84},{24,16},{28,92},{32,40}... | collective-permute-start | bytes 1376264 | tf_op jit(solution)/shard_map/ppermute | solution.py:131
  42.7 14.6 %all-to-all-done = bf16[4,96,2048]{2,1,0:T(8,128)(2,1)} async-done(((bf16[4,96,2048]{2,1,0:T(8,128)(2,1)}), bf16[4,96,2048]{2,1,0:T(8,128)(2,1)}, u32[]{:S(2)}, u32[]{:S(2)}) %all-to-all-start) | async-done | bytes 1572896 | tf_op jit(solution)/shard_map/all_to_all | solution.py:167
  57.4 2.3 %collective-permute-start.2 = (bf16[384,2048]{1,0:T(8,128)(2,1)}, bf16[384,2048]{1,0:T(8,128)(2,1)}, u32[]{:S(2)}, u32[]{:S(2)}) collective-permute-start(bf16[384,2048]{1,0:T(8,128)(2,1)} %bitcast.5.x_ref), channel_id=1, source_target_pairs={{0,4},{4,0},{8,12},{12,8},{16,20},{20,16},{24,28},{28,24},{32,36},... | collective-permute-start | bytes 4718600 | tf_op jit(solution)/shard_map/ppermute | solution.py:168
  59.7 7.9 %collective-permute-start.5 = (bf16[256,896]{1,0:T(8,128)(2,1)S(1)}, bf16[256,896]{1,0:T(8,128)(2,1)S(1)}, u32[]{:S(2)}, u32[]{:S(2)}) collective-permute-start(bf16[256,896]{1,0:T(8,128)(2,1)S(1)} %bitcast.19), channel_id=1, source_target_pairs={{0,56},{4,452},{8,16},{12,460},{16,8},{20,468},{24,32},{28,476},{3... | collective-permute-start | bytes 1376264 | tf_op jit(solution)/shard_map/ppermute | solution.py:132
  67.6 1.9 %collective-permute-start.7 = (bf16[256,896]{1,0:T(8,128)(2,1)S(1)}, bf16[256,896]{1,0:T(8,128)(2,1)S(1)}, u32[]{:S(2)}, u32[]{:S(2)}) collective-permute-start(bf16[256,896]{1,0:T(8,128)(2,1)S(1)} %collective-permute-done.4.e1), channel_id=1, source_target_pairs={{0,56},{4,452},{8,16},{12,460},{16,8},{20,468},{24,32},{28,476},{3... | collective-permute-start | bytes 1376264 | tf_op jit(solution)/shard_map/ppermute | solution.py:133
  69.6 4.2 %collective-permute-done.5.o1 = bf16[256,896]{1,0:T(8,128)(2,1)S(1)} collective-permute-done((bf16[256,896]{1,0:T(8,128)(2,1)S(1)}, bf16[256,896]{1,0:T(8,128)(2,1)S(1)}, u32[]{:S(2)}, u32[]{:S(2)}) %collective-permute-start.5) | collective-permute-done | bytes 458784 | tf_op jit(solution)/shard_map/ppermute | solution.py:132
  73.8 1.9 %collective-permute-start.6 = (bf16[256,896]{1,0:T(8,128)(2,1)S(1)}, bf16[256,896]{1,0:T(8,128)(2,1)S(1)}, u32[]{:S(2)}, u32[]{:S(2)}) collective-permute-start(bf16[256,896]{1,0:T(8,128)(2,1)S(1)} %collective-permute-done.5.o1), channel_id=1, source_target_pairs={{0,8},{4,68},{8,0},{12,76},{16,24},{20,84},{24,16},{28,92},{32,40}... | collective-permute-start | bytes 1376264 | tf_op jit(solution)/shard_map/ppermute | solution.py:134
  75.7 2.7 %collective-permute-done.7.o2 = bf16[256,896]{1,0:T(8,128)(2,1)S(1)} collective-permute-done((bf16[256,896]{1,0:T(8,128)(2,1)S(1)}, bf16[256,896]{1,0:T(8,128)(2,1)S(1)}, u32[]{:S(2)}, u32[]{:S(2)}) %collective-permute-start.7) | collective-permute-done | bytes 458784 | tf_op jit(solution)/shard_map/ppermute | solution.py:133
  78.4 1.9 %collective-permute-start.8 = (bf16[256,896]{1,0:T(8,128)(2,1)S(1)}, bf16[256,896]{1,0:T(8,128)(2,1)S(1)}, u32[]{:S(2)}, u32[]{:S(2)}) collective-permute-start(bf16[256,896]{1,0:T(8,128)(2,1)S(1)} %collective-permute-done.7.o2), channel_id=1, source_target_pairs={{0,8},{4,68},{8,0},{12,76},{16,24},{20,84},{24,16},{28,92},{32,40}... | collective-permute-start | bytes 1376264 | tf_op jit(solution)/shard_map/ppermute | solution.py:135
  80.3 2.9 %collective-permute-done.6.e2 = bf16[256,896]{1,0:T(8,128)(2,1)S(1)} collective-permute-done((bf16[256,896]{1,0:T(8,128)(2,1)S(1)}, bf16[256,896]{1,0:T(8,128)(2,1)S(1)}, u32[]{:S(2)}, u32[]{:S(2)}) %collective-permute-start.6) | collective-permute-done | bytes 458784 | tf_op jit(solution)/shard_map/ppermute | solution.py:134
  83.2 4.6 %collective-permute-start.9 = (bf16[256,896]{1,0:T(8,128)(2,1)S(1)}, bf16[256,896]{1,0:T(8,128)(2,1)S(1)}, u32[]{:S(2)}, u32[]{:S(2)}) collective-permute-start(bf16[256,896]{1,0:T(8,128)(2,1)S(1)} %collective-permute-done.6.e2), channel_id=1, source_target_pairs={{0,56},{4,452},{8,16},{12,460},{16,8},{20,468},{24,32},{28,476},{3... | collective-permute-start | bytes 1376264 | tf_op jit(solution)/shard_map/ppermute | solution.py:136
  88.2 4.6 %collective-permute-start.10 = (bf16[256,896]{1,0:T(8,128)(2,1)S(1)}, bf16[256,896]{1,0:T(8,128)(2,1)}, u32[]{:S(2)}, u32[]{:S(2)}) collective-permute-start(bf16[256,896]{1,0:T(8,128)(2,1)S(1)} %collective-permute-done.8.e3), channel_id=1, source_target_pairs={{0,56},{4,452},{8,16},{12,460},{16,8},{20,468},{24,32},{28,476},{3... | collective-permute-start | bytes 1376264 | tf_op jit(solution)/shard_map/ppermute | solution.py:137
  94.2 4.8 %collective-permute-done.10.o4 = bf16[256,896]{1,0:T(8,128)(2,1)} collective-permute-done((bf16[256,896]{1,0:T(8,128)(2,1)S(1)}, bf16[256,896]{1,0:T(8,128)(2,1)}, u32[]{:S(2)}, u32[]{:S(2)}) %collective-permute-start.10) | collective-permute-done | bytes 458784 | tf_op jit(solution)/shard_map/ppermute | solution.py:137
  99.1 10.3 %layer.1 = (bf16[256,2048]{1,0:T(8,128)(2,1)S(1)}, bf16[256,2048]{1,0:T(8,128)(2,1)}) custom-call(s32[4]{0:T(128)S(1)} %copy-done, f32[4]{0:T(128)S(1)} %copy-done.2, bf16[384,2048]{1,0:T(8,128)(2,1)} %bitcast.5.x_ref, bf16[384,2048]{1,0:T(8,128)(2,1)} %collective-permute-done.2.x2_ref, bf16[256,896]{1,0:T(8,128)(2,1)S(1)} %bitcast.20, ...), custom_call_target="tpu_custom_call" | custom-call | tf_op jit(solution)/shard_map/layer/pallas_call | solution.py:328
  109.4 3.3 %collective-permute-start.11 = (bf16[256,2048]{1,0:T(8,128)(2,1)}, bf16[256,2048]{1,0:T(8,128)(2,1)S(1)}, u32[]{:S(2)}, u32[]{:S(2)}) collective-permute-start(bf16[256,2048]{1,0:T(8,128)(2,1)} %get-tuple-element.14), channel_id=1, source_target_pairs={{0,4},{4,0},{8,12},{12,8},{16,20},{20,16},{24,28},{28,24},{32,36},... | collective-permute-start | bytes 3145736 | tf_op jit(solution)/shard_map/ppermute | solution.py:394
  112.7 2.5 %collective-permute-done.11 = bf16[256,2048]{1,0:T(8,128)(2,1)S(1)} collective-permute-done((bf16[256,2048]{1,0:T(8,128)(2,1)}, bf16[256,2048]{1,0:T(8,128)(2,1)S(1)}, u32[]{:S(2)}, u32[]{:S(2)}) %collective-permute-start.11) | collective-permute-done | bytes 1048608 | tf_op jit(solution)/shard_map/ppermute | solution.py:394
  115.6 17.2 %all_to_all.15 = bf16[4,64,2048]{2,1,0:T(8,128)(2,1)S(1)} all-to-all(bf16[4,64,2048]{2,1,0:T(8,128)(2,1)S(1)} %bitcast.23), channel_id=1, replica_groups=mesh['sp'=128,'tp'=4] {'tp'}, dimensions={0} | all-to-all | bytes 2097152 | tf_op jit(solution)/shard_map/all_to_all | solution.py:396
  (33 shorter events, 8.9 us)
Async XLA Ops:
  1.5 9.8 %collective-permute-start.3 = (bf16[16,1792]{1,0:T(8,128)(2,1)}, bf16[16,1792]{1,0:T(8,128)(2,1)S(1)}, u32[]{:S(2)}, u32[]{:S(2)}) collective-permute-start(bf16[16,1792]{1,0:T(8,128)(2,1)} %columns.1.mine_ref), channel_id=1, source_target_pairs={{0,4},{4,0},{8,12},{12,8},{16,20},{20,16},{24,28},{28,24},{32,36},... | collective-permute-start | bytes 172040 | tf_op jit(solution)/shard_map/ppermute | solution.py:127
  11.3 0.6 copy-start.7
  13.6 18.0 %all-to-all-start.1 = ((bf16[8,32,896]{2,1,0:T(8,128)(2,1)}), bf16[8,32,896]{2,1,0:T(8,128)(2,1)S(1)}, u32[]{:S(2)}, u32[]{:S(2)}) async-start(bf16[8,32,896]{2,1,0:T(8,128)(2,1)} %copies.1), calls=%async_computation.1 | async-start | bytes 917504 | tf_op jit(solution)/shard_map/all_to_all | solution.py:129
  19.0 2.0 %collective-permute-start = (bf16[32,2048]{1,0:T(8,128)(2,1)}, bf16[32,2048]{1,0:T(8,128)(2,1)S(1)}, u32[]{:S(2)}, u32[]{:S(2)}) collective-permute-start(bf16[32,2048]{1,0:T(8,128)(2,1)} %get-tuple-element.11), channel_id=1, source_target_pairs={{6,10},{7,11},{14,18},{15,19},{22,26},{23,27},{30,34},{31,35},{38,... | collective-permute-start | bytes 393224 | tf_op jit(solution)/shard_map/ppermute | solution.py:164
  19.6 8.9 %collective-permute-start.1 = (bf16[32,2048]{1,0:T(8,128)(2,1)}, bf16[32,2048]{1,0:T(8,128)(2,1)S(1)}, u32[]{:S(2)}, u32[]{:S(2)}) collective-permute-start(bf16[32,2048]{1,0:T(8,128)(2,1)} %get-tuple-element.12), channel_id=1, source_target_pairs={{6,14},{7,15},{14,22},{15,23},{22,30},{23,31},{30,38},{31,39},{38,... | collective-permute-start | bytes 393224 | tf_op jit(solution)/shard_map/ppermute | solution.py:165
  20.9 7.6 %copy-start.5 = (bf16[32,2048]{1,0:T(8,128)(2,1)}, bf16[32,2048]{1,0:T(8,128)(2,1)S(1)}, u32[]{:S(2)}) copy-start(bf16[32,2048]{1,0:T(8,128)(2,1)S(1)} %collective-permute-done.rim0) | copy-start | bytes 393220
  28.6 0.7 copy-start.6
  31.5 61.2 %copy-start.8 = (f32[128]{0:T(128)S(1)}, f32[128]{0:T(128)}, u32[]{:S(2)}) copy-start(f32[128]{0:T(128)} %constant.46.clone) | copy-start | bytes 1540
  31.5 67.5 %copy-start = (s32[4]{0:T(128)S(1)}, s32[4]{0:T(128)}, u32[]{:S(2)}) copy-start(s32[4]{0:T(128)} %pad_add_fusion.where_ref) | copy-start | bytes 52
  31.5 67.5 %copy-start.1 = (f32[3,256]{1,0:T(4,128)S(1)}, f32[3,256]{1,0:T(4,128)}, u32[]{:S(2)}) copy-start(f32[3,256]{1,0:T(4,128)} %conv_ref.1) | copy-start | bytes 9220
  31.5 67.5 %copy-start.2 = (f32[4]{0:T(128)S(1)}, f32[4]{0:T(128)}, u32[]{:S(2)}) copy-start(f32[4]{0:T(128)} %sink_ref.1) | copy-start | bytes 52
  31.5 67.5 %copy-start.3 = (f32[64]{0:T(128)S(1)}, f32[64]{0:T(128)}, u32[]{:S(2)}) copy-start(f32[64]{0:T(128)} %param.23) | copy-start | bytes 772
  31.6 67.5 %copy-start.4 = (f32[64]{0:T(128)S(1)}, f32[64]{0:T(128)}, u32[]{:S(2)}) copy-start(f32[64]{0:T(128)} %param.24) | copy-start | bytes 772
  31.6 25.8 %all-to-all-start = ((bf16[4,96,2048]{2,1,0:T(8,128)(2,1)}), bf16[4,96,2048]{2,1,0:T(8,128)(2,1)}, u32[]{:S(2)}, u32[]{:S(2)}) async-start(bf16[4,96,2048]{2,1,0:T(8,128)(2,1)} %rows.1), calls=%async_computation | async-start | bytes 3145728 | tf_op jit(solution)/shard_map/all_to_all | solution.py:167
  36.5 31.1 %collective-permute-start.4 = (bf16[256,896]{1,0:T(8,128)(2,1)S(1)}, bf16[256,896]{1,0:T(8,128)(2,1)S(1)}, u32[]{:S(2)}, u32[]{:S(2)}) collective-permute-start(bf16[256,896]{1,0:T(8,128)(2,1)S(1)} %bitcast.18), channel_id=1, source_target_pairs={{0,8},{4,68},{8,0},{12,76},{16,24},{20,84},{24,16},{28,92},{32,40}... | collective-permute-start | bytes 1376264 | tf_op jit(solution)/shard_map/ppermute | solution.py:131
  57.4 41.6 %collective-permute-start.2 = (bf16[384,2048]{1,0:T(8,128)(2,1)}, bf16[384,2048]{1,0:T(8,128)(2,1)}, u32[]{:S(2)}, u32[]{:S(2)}) collective-permute-start(bf16[384,2048]{1,0:T(8,128)(2,1)} %bitcast.5.x_ref), channel_id=1, source_target_pairs={{0,4},{4,0},{8,12},{12,8},{16,20},{20,16},{24,28},{28,24},{32,36},... | collective-permute-start | bytes 4718600 | tf_op jit(solution)/shard_map/ppermute | solution.py:168
  59.7 14.1 %collective-permute-start.5 = (bf16[256,896]{1,0:T(8,128)(2,1)S(1)}, bf16[256,896]{1,0:T(8,128)(2,1)S(1)}, u32[]{:S(2)}, u32[]{:S(2)}) collective-permute-start(bf16[256,896]{1,0:T(8,128)(2,1)S(1)} %bitcast.19), channel_id=1, source_target_pairs={{0,56},{4,452},{8,16},{12,460},{16,8},{20,468},{24,32},{28,476},{3... | collective-permute-start | bytes 1376264 | tf_op jit(solution)/shard_map/ppermute | solution.py:132
  67.6 10.8 %collective-permute-start.7 = (bf16[256,896]{1,0:T(8,128)(2,1)S(1)}, bf16[256,896]{1,0:T(8,128)(2,1)S(1)}, u32[]{:S(2)}, u32[]{:S(2)}) collective-permute-start(bf16[256,896]{1,0:T(8,128)(2,1)S(1)} %collective-permute-done.4.e1), channel_id=1, source_target_pairs={{0,56},{4,452},{8,16},{12,460},{16,8},{20,468},{24,32},{28,476},{3... | collective-permute-start | bytes 1376264 | tf_op jit(solution)/shard_map/ppermute | solution.py:133
  73.8 9.4 %collective-permute-start.6 = (bf16[256,896]{1,0:T(8,128)(2,1)S(1)}, bf16[256,896]{1,0:T(8,128)(2,1)S(1)}, u32[]{:S(2)}, u32[]{:S(2)}) collective-permute-start(bf16[256,896]{1,0:T(8,128)(2,1)S(1)} %collective-permute-done.5.o1), channel_id=1, source_target_pairs={{0,8},{4,68},{8,0},{12,76},{16,24},{20,84},{24,16},{28,92},{32,40}... | collective-permute-start | bytes 1376264 | tf_op jit(solution)/shard_map/ppermute | solution.py:134
  78.4 9.8 %collective-permute-start.8 = (bf16[256,896]{1,0:T(8,128)(2,1)S(1)}, bf16[256,896]{1,0:T(8,128)(2,1)S(1)}, u32[]{:S(2)}, u32[]{:S(2)}) collective-permute-start(bf16[256,896]{1,0:T(8,128)(2,1)S(1)} %collective-permute-done.7.o2), channel_id=1, source_target_pairs={{0,8},{4,68},{8,0},{12,76},{16,24},{20,84},{24,16},{28,92},{32,40}... | collective-permute-start | bytes 1376264 | tf_op jit(solution)/shard_map/ppermute | solution.py:135
  83.2 11.0 %collective-permute-start.9 = (bf16[256,896]{1,0:T(8,128)(2,1)S(1)}, bf16[256,896]{1,0:T(8,128)(2,1)S(1)}, u32[]{:S(2)}, u32[]{:S(2)}) collective-permute-start(bf16[256,896]{1,0:T(8,128)(2,1)S(1)} %collective-permute-done.6.e2), channel_id=1, source_target_pairs={{0,56},{4,452},{8,16},{12,460},{16,8},{20,468},{24,32},{28,476},{3... | collective-permute-start | bytes 1376264 | tf_op jit(solution)/shard_map/ppermute | solution.py:136
  88.2 10.8 %collective-permute-start.10 = (bf16[256,896]{1,0:T(8,128)(2,1)S(1)}, bf16[256,896]{1,0:T(8,128)(2,1)}, u32[]{:S(2)}, u32[]{:S(2)}) collective-permute-start(bf16[256,896]{1,0:T(8,128)(2,1)S(1)} %collective-permute-done.8.e3), channel_id=1, source_target_pairs={{0,56},{4,452},{8,16},{12,460},{16,8},{20,468},{24,32},{28,476},{3... | collective-permute-start | bytes 1376264 | tf_op jit(solution)/shard_map/ppermute | solution.py:137
  109.4 5.8 %collective-permute-start.11 = (bf16[256,2048]{1,0:T(8,128)(2,1)}, bf16[256,2048]{1,0:T(8,128)(2,1)S(1)}, u32[]{:S(2)}, u32[]{:S(2)}) collective-permute-start(bf16[256,2048]{1,0:T(8,128)(2,1)} %get-tuple-element.14), channel_id=1, source_target_pairs={{0,4},{4,0},{8,12},{12,8},{16,20},{20,16},{24,28},{28,24},{32,36},... | collective-permute-start | bytes 3145736 | tf_op jit(solution)/shard_map/ppermute | solution.py:394

commit v2 on v1

v2 whole, which is shorter than its diff:
```python
import jax
import jax.numpy as jnp
import numpy as np
from jax import lax
from jax.experimental import pallas as pl
from jax.experimental.pallas import tpu as pltpu
from jax.sharding import PartitionSpec as P


HEAD = 64
HALF = HEAD // 2
WINDOW = 128
BLOCK = 128
EPS = 1e-06
ROPE_BASE = 10000.0
NEG_FILL = -1e30
RING = 8
TP = 4
CHIPS = RING * RING
SP = 2 * CHIPS
LOCAL = 64
MAIN = TP * LOCAL
ROWS = MAIN + 2 * WINDOW
SHARE = 2 * LOCAL
PROJ = 1152
WIDTH = PROJ + 512


def sp_of(z, y, c):
    return (z * RING + y) * 2 + c


def even_partner(pos):
    return pos ^ 1


def odd_partner(pos):
    return (pos - 1) % RING if pos % 2 == 0 else (pos + 1) % RING


def matching(partner):
    pairs = []
    for z in range(RING):
        for y in range(RING):
            pairs.append((sp_of(z, y, 0), sp_of(z, partner(y), 0)))
            pairs.append((sp_of(z, y, 1), sp_of(partner(z), y, 1)))
    return pairs


EVEN = matching(even_partner)
ODD = matching(odd_partner)
SWAP = [(2 * k + c, 2 * k + 1 - c) for k in range(CHIPS) for c in range(2)]
GROUPS = [[sp_of(z, y, 0) for z in range(RING)] for y in range(RING)] + [
    [sp_of(z, y, 1) for y in range(RING)] for z in range(RING)
]
HALO = [(s * TP + x, (s + 1) * TP + x) for s in range(SP - 1) for x in (2, 3)] + [
    ((s + 1) * TP + x, s * TP + x) for s in range(SP - 1) for x in (0, 1)
]
MIB = 1024 * 1024
ANGLES = np.tile(ROPE_BASE ** (-np.arange(HALF) / HALF), 128 // HALF).astype(np.float32)
VMEM = pl.BlockSpec(memory_space=pltpu.VMEM)
SMEM = pl.BlockSpec(memory_space=pltpu.SMEM)


def copies_kernel(*refs):
    *weights, out = refs
    at = 0
    for ref in weights:
        width = ref.shape[1]
        for k in range(RING):
            out[k, :, at : at + width] = ref[...]
        at += width


def copies(weights):
    return pl.pallas_call(
        copies_kernel,
        out_shape=jax.ShapeDtypeStruct((RING, weights[0].shape[1], WIDTH), jnp.bfloat16),
        in_specs=[VMEM] * len(weights),
        out_specs=VMEM,
        name="copies",
    )(*[w.T for w in weights])


def rows_kernel(normed, rim, out):
    for x in range(TP):
        out[x, :LOCAL, :] = normed[...]
        out[x, LOCAL:, :] = rim[...]


def row_copies(normed, rim):
    return pl.pallas_call(
        rows_kernel,
        out_shape=jax.ShapeDtypeStruct((TP, SHARE, normed.shape[1]), jnp.bfloat16),
        in_specs=[VMEM] * 2,
        out_specs=VMEM,
        compiler_params=pltpu.CompilerParams(vmem_limit_bytes=8 * MIB),
    name="rows",
    )(normed, rim)


def gathered_weights(weights):
    blocks = copies(weights)
    own = lax.all_to_all(blocks, "sp", 0, 0, axis_index_groups=GROUPS, tiled=True)
    own = own.reshape(-1, WIDTH)
    e1 = lax.ppermute(own, "sp", EVEN)
    o1 = lax.ppermute(own, "sp", ODD)
    o2 = lax.ppermute(e1, "sp", ODD)
    e2 = lax.ppermute(o1, "sp", EVEN)
    e3 = lax.ppermute(o2, "sp", EVEN)
    o3 = lax.ppermute(e2, "sp", ODD)
    o4 = lax.ppermute(e3, "sp", ODD)
    first = packed((own, e1, o1, o2))
    second = packed((e2, e3, o3))
    kept = (first, second, o4)
    return kept + tuple(lax.ppermute(p, "sp", SWAP) for p in kept)


def packed(pieces):
    def body(*refs):
        *sources, out = refs
        for k, ref in enumerate(sources):
            out[k * 128 : (k + 1) * 128, :] = ref[...]

    return pl.pallas_call(
        body,
        out_shape=jax.ShapeDtypeStruct((128 * len(pieces), WIDTH), jnp.bfloat16),
        in_specs=[VMEM] * len(pieces),
        out_specs=VMEM,
        compiler_params=pltpu.CompilerParams(vmem_limit_bytes=8 * MIB),
    )(*pieces)


def norm_kernel(x_ref, gain_ref, normed):
    wide = x_ref[...].astype(jnp.float32)
    mean = jnp.mean(wide * wide, axis=-1, keepdims=True)
    normed[...] = (wide * lax.rsqrt(mean + EPS) * gain_ref[...]).astype(jnp.bfloat16)


def normalized(tokens, norm_gain):
    return pl.pallas_call(
        norm_kernel,
        out_shape=jax.ShapeDtypeStruct(tokens.shape, jnp.bfloat16),
        in_specs=[VMEM] * 2,
        out_specs=VMEM,
        name="norm",
    )(tokens, norm_gain[None])


def gathered_tokens(normed):
    rim = lax.ppermute(normed, ("sp", "tp"), HALO)
    sent = row_copies(normed, rim)
    return lax.all_to_all(sent, "tp", 0, 0, tiled=True)


PIECE_STEPS = (0, 1, -1, -2, 2, 3, -3, -4)


def layer_kernel(where_ref, sink_ref, x_ref, *refs):
    pieces = []
    for first, second, third in (refs[:3], refs[3:6]):
        pieces += [(first, k * 128) for k in range(4)]
        pieces += [(second, k * 128) for k in range(3)] + [(third, 0)]
    cos_ref, sin_ref, qg_ref, kg_ref, conv_ref, out_ref = refs[6:12]
    w_s, p_s, kk_s, vv_s, prod_s, act_s = refs[12:]
    core, y, z, place = where_ref[0], where_ref[1], where_ref[2], where_ref[3]

    for k, (piece, base) in enumerate(pieces):
        owner = core if k < 8 else 1 - core
        pos = jnp.where(owner == 0, y, z)
        sgn = 1 - 2 * lax.rem(pos, 2)
        at = lax.rem(pos + sgn * PIECE_STEPS[k % 8] + 2 * RING, RING)
        for j in range(RING):
            to = jnp.where(owner == 0, j * 256 + at * 32, at * 256 + j * 32 + 16)
            w_s[pl.ds(pl.multiple_of(to, 16), 16), :] = piece[
                base + j * 16 : base + (j + 1) * 16, :
            ]

    features = x_ref.shape[-1]
    main = x_ref[:, :LOCAL, :].reshape(MAIN, features)
    rim = x_ref[:, LOCAL:, :].reshape(MAIN, features)
    for lo in range(0, PROJ, 128):
        cols = slice(lo, lo + 128)
        part = jnp.dot(main, w_s[:, cols], preferred_element_type=jnp.float32)
        p_s[WINDOW : WINDOW + MAIN, cols] = part.astype(jnp.bfloat16)
        if lo < 256 or 384 <= lo < 640:
            continue
        part = jnp.dot(rim, w_s[:, cols], preferred_element_type=jnp.float32).astype(jnp.bfloat16)
        p_s[:WINDOW, cols] = part[WINDOW:]
        p_s[WINDOW + MAIN :, cols] = part[:WINDOW]

    def gain_rows(ref, scale):
        gain = jnp.concatenate([ref[...], ref[...]], axis=1) * scale
        lane = lax.rem(lax.broadcasted_iota(jnp.int32, gain.shape, 1), HEAD)
        low = pltpu.roll(gain, 128 - HALF, 1)
        return gain, jnp.where(lane < HALF, -low, pltpu.roll(gain, HALF, 1))

    query_gain = gain_rows(qg_ref, HEAD ** (-0.5))
    key_gain = gain_rows(kg_ref, 1.0)

    def rotated(value, at, gain, crossed_gain):
        lane = lax.broadcasted_iota(jnp.int32, value.shape, 1)
        low = lane < HEAD
        square = value * value
        mean0 = jnp.sum(jnp.where(low, square, 0.0), axis=-1, keepdims=True) * (1.0 / HEAD)
        mean1 = jnp.sum(jnp.where(low, 0.0, square), axis=-1, keepdims=True) * (1.0 / HEAD)
        scaled = value * jnp.where(low, lax.rsqrt(mean0 + EPS), lax.rsqrt(mean1 + EPS))
        crossed = jnp.where(
            lax.rem(lane, HEAD) < HALF,
            pltpu.roll(scaled, 2 * HEAD - HALF, 1),
            pltpu.roll(scaled, HALF, 1),
        )
        cosine = cos_ref[at : at + BLOCK, :]
        sine = sin_ref[at : at + BLOCK, :]
        return scaled * (cosine * gain) + crossed * (sine * crossed_gain)

    for at in range(0, ROWS, BLOCK):
        kv = p_s[at : at + BLOCK, 256:384].astype(jnp.float32)
        lane = lax.broadcasted_iota(jnp.int32, kv.shape, 1)
        key = rotated(kv, at, *key_gain)
        kk_s[at : at + BLOCK, :] = jnp.where(lane < HEAD, key, pltpu.roll(key, HEAD, 1)).astype(
            jnp.bfloat16
        )
        vv_s[at : at + BLOCK, :] = jnp.where(lane < HEAD, pltpu.roll(kv, HEAD, 1), kv).astype(
            jnp.bfloat16
        )
        prod_s[at : at + BLOCK, :] = (
            (
                p_s[at : at + BLOCK, 640:896].astype(jnp.float32)
                * p_s[at : at + BLOCK, 896:1152].astype(jnp.float32)
            )
            .astype(jnp.bfloat16)
            .astype(jnp.float32)
        )

    for at in range(0, MAIN, BLOCK):
        rows = slice(at + WINDOW, at + WINDOW + BLOCK)
        keys = kk_s[at : at + 3 * BLOCK, :]
        values = vv_s[at : at + 3 * BLOCK, :]
        shape = (BLOCK, 3 * BLOCK)
        q_at = lax.broadcasted_iota(jnp.int32, shape, 0)
        k_at = lax.broadcasted_iota(jnp.int32, shape, 1) - WINDOW
        k_pos = k_at + (place * MAIN + at)
        allowed = (jnp.abs(q_at - k_at) <= WINDOW) & (k_pos >= 0) & (k_pos < SP * MAIN)
        for pair in range(2):
            lanes = slice(pair * 128, (pair + 1) * 128)
            query = rotated(p_s[rows, lanes].astype(jnp.float32), at + WINDOW, *query_gain)
            low = lax.broadcasted_iota(jnp.int32, query.shape, 1) < HEAD
            outs = []
            for head in range(2):
                q_head = jnp.where(low if head == 0 else ~low, query, 0.0).astype(jnp.bfloat16)
                scores = lax.dot_general(
                    q_head, keys, (((1,), (1,)), ((), ())), preferred_element_type=jnp.float32
                )
                scores = jnp.where(allowed, scores, NEG_FILL)
                sink = sink_ref[2 * pair + head]
                top = jnp.maximum(jnp.max(scores, axis=-1, keepdims=True), sink)
                expo = jnp.exp(scores - top)
                total = jnp.sum(expo, axis=-1, keepdims=True) + jnp.exp(sink - top)
                weights = (expo * (1.0 / total)).astype(jnp.bfloat16)
                outs.append(jnp.dot(weights, values, preferred_element_type=jnp.float32))
            act_s[at : at + BLOCK, lanes] = jnp.where(low, outs[0], outs[1]).astype(jnp.bfloat16)
        lo = at + WINDOW
        mixed = (
            conv_ref[0:1, :] * prod_s[lo - 1 : lo - 1 + BLOCK, :]
            + conv_ref[1:2, :] * prod_s[lo : lo + BLOCK, :]
            + conv_ref[2:3, :] * prod_s[lo + 1 : lo + 1 + BLOCK, :]
        )
        act_s[at : at + BLOCK, 256:512] = (p_s[rows, 384:640].astype(jnp.float32) * mixed).astype(
            jnp.bfloat16
        )

    for lo in range(0, features, 256):
        out_ref[:, lo : lo + 256] = lax.dot_general(
            act_s[...],
            w_s[lo : lo + 256, PROJ:],
            (((1,), (1,)), ((), ())),
            preferred_element_type=jnp.float32,
        ).astype(jnp.bfloat16)


def run_layer(where, sinks, tokens, pieces, tables, conv):
    features = tokens.shape[-1]
    return pl.pallas_call(
        layer_kernel,
        out_shape=jax.ShapeDtypeStruct((MAIN, features), jnp.bfloat16),
        in_specs=[SMEM, SMEM] + [VMEM] * (1 + len(pieces) + len(tables) + 1),
        out_specs=VMEM,
        scratch_shapes=[
            pltpu.VMEM((features, WIDTH), jnp.bfloat16),
            pltpu.VMEM((ROWS, PROJ), jnp.bfloat16),
            pltpu.VMEM((ROWS, 128), jnp.bfloat16),
            pltpu.VMEM((ROWS, 128), jnp.bfloat16),
            pltpu.VMEM((ROWS, 256), jnp.float32),
            pltpu.VMEM((MAIN, 512), jnp.bfloat16),
        ],
        compiler_params=pltpu.CompilerParams(vmem_limit_bytes=32 * MIB),
        name="layer",
    )(where, sinks, tokens, *pieces, *tables, conv)


def per_device(
    tokens,
    norm_gain,
    query_weight,
    key_weight,
    value_weight,
    gate_weight,
    left_weight,
    input_weight,
    query_gain,
    key_gain,
    sink_logit,
    conv_weight,
    out_attention,
    out_conv,
):
    place = lax.axis_index("sp").astype(jnp.int32)
    where = jnp.stack([lax.rem(place, 2), lax.rem(place // 2, RING), place // (2 * RING), place])
    gathered = gathered_tokens(normalized(tokens, norm_gain))
    pieces = gathered_weights(
        (
            query_weight,
            key_weight,
            value_weight,
            gate_weight,
            left_weight,
            input_weight,
            out_attention,
            out_conv,
        )
    )
    positions = (place * MAIN - WINDOW + jnp.arange(ROWS, dtype=jnp.int32)).astype(jnp.float32)
    angle = positions[:, None] * ANGLES
    tables = (jnp.cos(angle), jnp.sin(angle), query_gain[None], key_gain[None])
    partial = run_layer(where, sink_logit, gathered, pieces, tables, conv_weight)
    blocks = lax.all_to_all(partial.reshape(TP, LOCAL, -1), "tp", 0, 0, tiled=True)
    return blocks.astype(jnp.float32).sum(axis=0).astype(jnp.bfloat16)


def solution(mesh):
    in_specs = (
        P(("sp", "tp"), None),
        P(),
        P("tp", "sp"),
        P("tp", "sp"),
        P("tp", "sp"),
        P("tp", "sp"),
        P("tp", "sp"),
        P("tp", "sp"),
        P(),
        P(),
        P("tp"),
        P(None, "tp"),
        P("tp", "sp"),
        P("tp", "sp"),
    )
    out_specs = P(("sp", "tp"), None)

    return jax.shard_map(
        per_device, mesh=mesh, in_specs=in_specs, out_specs=out_specs, check_vma=False
    )
```

time: 134 us -> 122 us (0.910)
  the two profiles are of different devices: /device:TPU:1 before, /device:TPU:17 now
where the time goes in v2:
time: 122 us; the launch traced here: 119 us
  starting transfers between devices  42.9 us (35%)
  blocking collectives  31.6 us (26%)
  waiting for transfers between devices  19.1 us (16%)
  Pallas kernels  18 us (15%)
  local copies, waits for them, and re-layouts  4.7 us (4%)
  other arithmetic  2.8 us (2%)
    all_to_all x1, blocking collectives, per_device(): lax.all_to_all(partial.reshape(TP, LOCAL, -1), 'tp', 0, 0, tiled=True)  16.5 us
    all_to_all x1, blocking collectives, gathered_weights(): lax.all_to_all(blocks, 'sp', 0, 0, axis_index_groups=GROUPS, tiled=True)  15.2 us
    ppermute x3, starting transfers between devices, gathered_weights(): return kept + tuple((lax.ppermute(p, 'sp', SWAP) for p in kept))  10.8 us
    pallas_call x1, Pallas kernels, run_layer(): pl.pallas_call(layer_kernel, out_shape=jax.ShapeDtypeStruct((MAIN, featur...  10.7 us
    ppermute x1, starting transfers between devices, gathered_weights(): o1 = lax.ppermute(own, 'sp', ODD)  10.7 us
    ppermute x1, waiting for transfers between devices, gathered_weights(): o4 = lax.ppermute(e3, 'sp', ODD)  8.13 us
    all_to_all x1, waiting for transfers between devices, gathered_tokens(): return lax.all_to_all(sent, 'tp', 0, 0, tiled=True)  5.65 us
    unnamed x24, local copies, waits for them, and re-layouts  4.7 us
  transfers between devices with their start and end apart: 12, of which 4 were waited for; matrix products, arithmetic and copies ran while one was open for 2% of the time, Pallas kernels for 5%

profile of v2, /device:TPU:17, one launch (start us, length us, event | category | flops | bytes accessed | tf_op | source)
XLA Modules:
  0.0 119.4 jit_solution(5726519122537982048)
XLA Ops:
  0.0 1.6 %copies.1 = bf16[8,16,1664]{2,1,0:T(8,128)(2,1)} custom-call(bf16[16,256]{1,0:T(8,128)(2,1)} %bitcast.23, bf16[16,64]{1,0:T(8,128)(2,1)} %bitcast.30, bf16[16,64]{1,0:T(8,128)(2,1)} %bitcast.31, bf16[16,256]{1,0:T(8,128)(2,1)} %bitcast.24, bf16[16,256]{1,0:T(8,128)(2,1)} %bitcast.25, bf16[16,256]{1,0:T(8,128)(2,1)} %bitcast.26, bf16[16,256]{1,0:T(8,128)(2,1)} %bitcast.27, ...), custom_call_target="tpu_custom_call" | custom-call | tf_op jit(solution)/shard_map/copies/pallas_call | solution.py:76
  1.6 15.2 %all_to_all.15 = bf16[8,16,1664]{2,1,0:T(8,128)(2,1)S(1)} all-to-all(bf16[8,16,1664]{2,1,0:T(8,128)(2,1)} %copies.1), channel_id=1, replica_groups={{0,64,128,192,256,320,384,448},{8,72,136,200,264,328,392,456},{16,80,14..., dimensions={0} | all-to-all | bytes 851968 | tf_op jit(solution)/shard_map/all_to_all | solution.py:104
  16.8 10.7 %collective-permute-start.2 = (bf16[128,1664]{1,0:T(8,128)(2,1)S(1)}, bf16[128,1664]{1,0:T(8,128)(2,1)S(1)}, u32[]{:S(2)}, u32[]{:S(2)}) collective-permute-start(bf16[128,1664]{1,0:T(8,128)(2,1)S(1)} %bitcast.18), channel_id=1, source_target_pairs={{0,56},{4,452},{8,16},{12,460},{16,8},{20,468},{24,32},{28,476},{3... | collective-permute-start | bytes 1277960 | tf_op jit(solution)/shard_map/ppermute | solution.py:107
  27.5 1.9 %collective-permute-start.1 = (bf16[128,1664]{1,0:T(8,128)(2,1)S(1)}, bf16[128,1664]{1,0:T(8,128)(2,1)S(1)}, u32[]{:S(2)}, u32[]{:S(2)}) collective-permute-start(bf16[128,1664]{1,0:T(8,128)(2,1)S(1)} %bitcast.19), channel_id=1, source_target_pairs={{0,8},{4,68},{8,0},{12,76},{16,24},{20,84},{24,16},{28,92},{32,40}... | collective-permute-start | bytes 1277960 | tf_op jit(solution)/shard_map/ppermute | solution.py:106
  29.4 3.6 %collective-permute-done.2.refs_2_ = bf16[128,1664]{1,0:T(8,128)(2,1)S(1)} collective-permute-done((bf16[128,1664]{1,0:T(8,128)(2,1)S(1)}, bf16[128,1664]{1,0:T(8,128)(2,1)S(1)}, u32[]{:S(2)}, u32[]{:S(2)}) %collective-permute-start.2) | collective-permute-done | bytes 426016 | tf_op jit(solution)/shard_map/ppermute | solution.py:107
  33.0 1.9 %collective-permute-start.4 = (bf16[128,1664]{1,0:T(8,128)(2,1)S(1)}, bf16[128,1664]{1,0:T(8,128)(2,1)S(1)}, u32[]{:S(2)}, u32[]{:S(2)}) collective-permute-start(bf16[128,1664]{1,0:T(8,128)(2,1)S(1)} %collective-permute-done.2.refs_2_), channel_id=1, source_target_pairs={{0,8},{4,68},{8,0},{12,76},{16,24},{20,84},{24,16},{28,92},{32,40}... | collective-permute-start | bytes 1277960 | tf_op jit(solution)/shard_map/ppermute | solution.py:109
  34.9 1.7 %collective-permute-done.1.refs_1_ = bf16[128,1664]{1,0:T(8,128)(2,1)S(1)} collective-permute-done((bf16[128,1664]{1,0:T(8,128)(2,1)S(1)}, bf16[128,1664]{1,0:T(8,128)(2,1)S(1)}, u32[]{:S(2)}, u32[]{:S(2)}) %collective-permute-start.1) | collective-permute-done | bytes 426016 | tf_op jit(solution)/shard_map/ppermute | solution.py:106
  36.6 2.8 %collective-permute-start.3 = (bf16[128,1664]{1,0:T(8,128)(2,1)S(1)}, bf16[128,1664]{1,0:T(8,128)(2,1)S(1)}, u32[]{:S(2)}, u32[]{:S(2)}) collective-permute-start(bf16[128,1664]{1,0:T(8,128)(2,1)S(1)} %collective-permute-done.1.refs_1_), channel_id=1, source_target_pairs={{0,56},{4,452},{8,16},{12,460},{16,8},{20,468},{24,32},{28,476},{3... | collective-permute-start | bytes 1277960 | tf_op jit(solution)/shard_map/ppermute | solution.py:108
  39.5 1.8 %norm.1.normed = bf16[64,2048]{1,0:T(8,128)(2,1)} custom-call(bf16[64,2048]{1,0:T(8,128)(2,1)} %x_ref.1, f32[1,2048]{1,0:T(1,128)} %bitcast.29), custom_call_target="tpu_custom_call" | custom-call | tf_op jit(solution)/shard_map/norm/pallas_call | solution.py:141
  41.3 4.1 %collective-permute-start = (bf16[64,2048]{1,0:T(8,128)(2,1)}, bf16[64,2048]{1,0:T(8,128)(2,1)S(1)}, u32[]{:S(2)}, u32[]{:S(2)}) collective-permute-start(bf16[64,2048]{1,0:T(8,128)(2,1)} %norm.1.normed), channel_id=1, source_target_pairs={{2,6},{3,7},{6,10},{7,11},{10,14},{11,15},{14,18},{15,19},{18,22},... | collective-permute-start | bytes 786440 | tf_op jit(solution)/shard_map/ppermute | solution.py:151
  45.4 1.9 %collective-permute-start.6 = (bf16[128,1664]{1,0:T(8,128)(2,1)S(1)}, bf16[128,1664]{1,0:T(8,128)(2,1)S(1)}, u32[]{:S(2)}, u32[]{:S(2)}) collective-permute-start(bf16[128,1664]{1,0:T(8,128)(2,1)S(1)} %collective-permute-done.4.refs_0_), channel_id=1, source_target_pairs={{0,56},{4,452},{8,16},{12,460},{16,8},{20,468},{24,32},{28,476},{3... | collective-permute-start | bytes 1277960 | tf_op jit(solution)/shard_map/ppermute | solution.py:111
  47.3 2.2 %collective-permute-start.5 = (bf16[128,1664]{1,0:T(8,128)(2,1)S(1)}, bf16[128,1664]{1,0:T(8,128)(2,1)}, u32[]{:S(2)}, u32[]{:S(2)}) collective-permute-start(bf16[128,1664]{1,0:T(8,128)(2,1)S(1)} %collective-permute-done.3.refs_3_), channel_id=1, source_target_pairs={{0,8},{4,68},{8,0},{12,76},{16,24},{20,84},{24,16},{28,92},{32,40}... | collective-permute-start | bytes 1277960 | tf_op jit(solution)/shard_map/ppermute | solution.py:110
  49.5 1.3 %shard_map.145.refs_0_ = bf16[512,1664]{1,0:T(8,128)(2,1)} custom-call(bf16[128,1664]{1,0:T(8,128)(2,1)S(1)} %bitcast.20, bf16[128,1664]{1,0:T(8,128)(2,1)S(1)} %collective-permute-done.1.refs_1_, bf16[128,1664]{1,0:T(8,128)(2,1)S(1)} %collective-permute-done.2.refs_2_, bf16[128,1664]{1,0:T(8,128)(2,1)S(1)} %collective-permute-done.3.refs_3_), custom_call_target="tpu_custom_call" | custom-call | tf_op jit(solution)/shard_map/pallas_call | solution.py:125
  50.8 6.7 %collective-permute-start.8 = (bf16[512,1664]{1,0:T(8,128)(2,1)}, bf16[512,1664]{1,0:T(8,128)(2,1)}, u32[]{:S(2)}, u32[]{:S(2)}) collective-permute-start(bf16[512,1664]{1,0:T(8,128)(2,1)} %shard_map.145.refs_0_), channel_id=1, source_target_pairs={{0,4},{4,0},{8,12},{12,8},{16,20},{20,16},{24,28},{28,24},{32,36},... | collective-permute-start | bytes 5111816 | tf_op jit(solution)/shard_map/ppermute | solution.py:116
  57.5 1.5 %rows.1 = bf16[4,128,2048]{2,1,0:T(8,128)(2,1)} custom-call(bf16[64,2048]{1,0:T(8,128)(2,1)S(1)} %copy-done.2, bf16[64,2048]{1,0:T(8,128)(2,1)S(1)} %collective-permute-done.rim), custom_call_target="tpu_custom_call" | custom-call | tf_op jit(solution)/shard_map/rows/pallas_call | solution.py:92
  59.0 4.2 %all-to-all-start = ((bf16[4,128,2048]{2,1,0:T(8,128)(2,1)}), bf16[4,128,2048]{2,1,0:T(8,128)(2,1)S(1)}, u32[]{:S(2)}, u32[]{:S(2)}) async-start(bf16[4,128,2048]{2,1,0:T(8,128)(2,1)} %rows.1), calls=%async_computation | async-start | bytes 4194304 | tf_op jit(solution)/shard_map/all_to_all | solution.py:153
  67.1 2.2 %collective-permute-start.9 = (bf16[384,1664]{1,0:T(8,128)(2,1)S(1)}, bf16[384,1664]{1,0:T(8,128)(2,1)}, u32[]{:S(2)}, u32[]{:S(2)}) collective-permute-start(bf16[384,1664]{1,0:T(8,128)(2,1)S(1)} %shard_map.146.refs_1_), channel_id=1, source_target_pairs={{0,4},{4,0},{8,12},{12,8},{16,20},{20,16},{24,28},{28,24},{32,36},... | collective-permute-start | bytes 3833864 | tf_op jit(solution)/shard_map/ppermute | solution.py:116
  69.3 2.4 %collective-permute-start.7 = (bf16[128,1664]{1,0:T(8,128)(2,1)}, bf16[128,1664]{1,0:T(8,128)(2,1)}, u32[]{:S(2)}, u32[]{:S(2)}) collective-permute-start(bf16[128,1664]{1,0:T(8,128)(2,1)} %collective-permute-done.5.refs_1_), channel_id=1, source_target_pairs={{0,56},{4,452},{8,16},{12,460},{16,8},{20,468},{24,32},{28,476},{3... | collective-permute-start | bytes 1277960 | tf_op jit(solution)/shard_map/ppermute | solution.py:112
  71.7 8.1 %collective-permute-done.7.refs_2_ = bf16[128,1664]{1,0:T(8,128)(2,1)} collective-permute-done((bf16[128,1664]{1,0:T(8,128)(2,1)}, bf16[128,1664]{1,0:T(8,128)(2,1)}, u32[]{:S(2)}, u32[]{:S(2)}) %collective-permute-start.7) | collective-permute-done | bytes 426016 | tf_op jit(solution)/shard_map/ppermute | solution.py:112
  79.9 1.9 %collective-permute-start.10 = (bf16[128,1664]{1,0:T(8,128)(2,1)}, bf16[128,1664]{1,0:T(8,128)(2,1)}, u32[]{:S(2)}, u32[]{:S(2)}) collective-permute-start(bf16[128,1664]{1,0:T(8,128)(2,1)} %collective-permute-done.7.refs_2_), channel_id=1, source_target_pairs={{0,4},{4,0},{8,12},{12,8},{16,20},{20,16},{24,28},{28,24},{32,36},... | collective-permute-start | bytes 1277960 | tf_op jit(solution)/shard_map/ppermute | solution.py:116
  81.9 1.8 %multiply_sine_fusion = (f32[512,128]{1,0:T(8,128)}, f32[512,128]{1,0:T(8,128)}) fusion(f32[128]{0:T(128)S(1)} %copy-done.11, f32[512]{0:T(512)S(1)} %add_convert_fusion), kind=kLoop, calls=%fused_computation | loop fusion | flops 65536 | bytes 526848 | tf_op jit(solution)/shard_map/sin | solution.py:335
  83.7 5.6 %all-to-all-done.x_ref = bf16[4,128,2048]{2,1,0:T(8,128)(2,1)S(1)} async-done(((bf16[4,128,2048]{2,1,0:T(8,128)(2,1)}), bf16[4,128,2048]{2,1,0:T(8,128)(2,1)S(1)}, u32[]{:S(2)}, u32[]{:S(2)}) %all-to-all-start) | async-done | bytes 2097184 | tf_op jit(solution)/shard_map/all_to_all | solution.py:153
  91.3 10.7 %layer.1 = bf16[256,2048]{1,0:T(8,128)(2,1)S(1)} custom-call(s32[4]{0:T(128)S(1)} %pad_add_fusion.where_ref, f32[4]{0:T(128)S(1)} %copy-done.8, bf16[4,128,2048]{2,1,0:T(8,128)(2,1)S(1)} %all-to-all-done.x_ref, bf16[512,1664]{1,0:T(8,128)(2,1)} %shard_map.145.refs_0_, bf16[384,1664]{1,0:T(8,128)(2,1)S(1)} %shard_map.146.refs_1_, ...), custom_call_target="tpu_custom_call" | custom-call | tf_op jit(solution)/shard_map/layer/pallas_call | solution.py:284
  102.0 16.5 %all_to_all.16 = bf16[4,64,2048]{2,1,0:T(8,128)(2,1)S(1)} all-to-all(bf16[4,64,2048]{2,1,0:T(8,128)(2,1)S(1)} %bitcast.17), channel_id=1, replica_groups=mesh['sp'=128,'tp'=4] {'tp'}, dimensions={0} | all-to-all | bytes 2097152 | tf_op jit(solution)/shard_map/all_to_all | solution.py:337
  (36 shorter events, 6.8 us)
Async XLA Ops:
  16.8 16.2 %collective-permute-start.2 = (bf16[128,1664]{1,0:T(8,128)(2,1)S(1)}, bf16[128,1664]{1,0:T(8,128)(2,1)S(1)}, u32[]{:S(2)}, u32[]{:S(2)}) collective-permute-start(bf16[128,1664]{1,0:T(8,128)(2,1)S(1)} %bitcast.18), channel_id=1, source_target_pairs={{0,56},{4,452},{8,16},{12,460},{16,8},{20,468},{24,32},{28,476},{3... | collective-permute-start | bytes 1277960 | tf_op jit(solution)/shard_map/ppermute | solution.py:107
  27.5 9.2 %collective-permute-start.1 = (bf16[128,1664]{1,0:T(8,128)(2,1)S(1)}, bf16[128,1664]{1,0:T(8,128)(2,1)S(1)}, u32[]{:S(2)}, u32[]{:S(2)}) collective-permute-start(bf16[128,1664]{1,0:T(8,128)(2,1)S(1)} %bitcast.19), channel_id=1, source_target_pairs={{0,8},{4,68},{8,0},{12,76},{16,24},{20,84},{24,16},{28,92},{32,40}... | collective-permute-start | bytes 1277960 | tf_op jit(solution)/shard_map/ppermute | solution.py:106
  33.0 12.4 %collective-permute-start.4 = (bf16[128,1664]{1,0:T(8,128)(2,1)S(1)}, bf16[128,1664]{1,0:T(8,128)(2,1)S(1)}, u32[]{:S(2)}, u32[]{:S(2)}) collective-permute-start(bf16[128,1664]{1,0:T(8,128)(2,1)S(1)} %collective-permute-done.2.refs_2_), channel_id=1, source_target_pairs={{0,8},{4,68},{8,0},{12,76},{16,24},{20,84},{24,16},{28,92},{32,40}... | collective-permute-start | bytes 1277960 | tf_op jit(solution)/shard_map/ppermute | solution.py:109
  36.6 10.7 %collective-permute-start.3 = (bf16[128,1664]{1,0:T(8,128)(2,1)S(1)}, bf16[128,1664]{1,0:T(8,128)(2,1)S(1)}, u32[]{:S(2)}, u32[]{:S(2)}) collective-permute-start(bf16[128,1664]{1,0:T(8,128)(2,1)S(1)} %collective-permute-done.1.refs_1_), channel_id=1, source_target_pairs={{0,56},{4,452},{8,16},{12,460},{16,8},{20,468},{24,32},{28,476},{3... | collective-permute-start | bytes 1277960 | tf_op jit(solution)/shard_map/ppermute | solution.py:108
  41.3 16.2 %copy-start.2 = (bf16[64,2048]{1,0:T(8,128)(2,1)S(1)}, bf16[64,2048]{1,0:T(8,128)(2,1)}, u32[]{:S(2)}) copy-start(bf16[64,2048]{1,0:T(8,128)(2,1)} %norm.1.normed) | copy-start | bytes 786436
  41.3 16.2 %collective-permute-start = (bf16[64,2048]{1,0:T(8,128)(2,1)}, bf16[64,2048]{1,0:T(8,128)(2,1)S(1)}, u32[]{:S(2)}, u32[]{:S(2)}) collective-permute-start(bf16[64,2048]{1,0:T(8,128)(2,1)} %norm.1.normed), channel_id=1, source_target_pairs={{2,6},{3,7},{6,10},{7,11},{10,14},{11,15},{14,18},{15,19},{18,22},... | collective-permute-start | bytes 786440 | tf_op jit(solution)/shard_map/ppermute | solution.py:151
  45.4 5.5 %copy-start.3 = (bf16[128,1664]{1,0:T(8,128)(2,1)}, bf16[128,1664]{1,0:T(8,128)(2,1)S(1)}, u32[]{:S(2)}) copy-start(bf16[128,1664]{1,0:T(8,128)(2,1)S(1)} %collective-permute-done.4.refs_0_) | copy-start | bytes 1277956
  45.4 17.8 %collective-permute-start.6 = (bf16[128,1664]{1,0:T(8,128)(2,1)S(1)}, bf16[128,1664]{1,0:T(8,128)(2,1)S(1)}, u32[]{:S(2)}, u32[]{:S(2)}) collective-permute-start(bf16[128,1664]{1,0:T(8,128)(2,1)S(1)} %collective-permute-done.4.refs_0_), channel_id=1, source_target_pairs={{0,56},{4,452},{8,16},{12,460},{16,8},{20,468},{24,32},{28,476},{3... | collective-permute-start | bytes 1277960 | tf_op jit(solution)/shard_map/ppermute | solution.py:111
  47.3 16.6 %collective-permute-start.5 = (bf16[128,1664]{1,0:T(8,128)(2,1)S(1)}, bf16[128,1664]{1,0:T(8,128)(2,1)}, u32[]{:S(2)}, u32[]{:S(2)}) collective-permute-start(bf16[128,1664]{1,0:T(8,128)(2,1)S(1)} %collective-permute-done.3.refs_3_), channel_id=1, source_target_pairs={{0,8},{4,68},{8,0},{12,76},{16,24},{20,84},{24,16},{28,92},{32,40}... | collective-permute-start | bytes 1277960 | tf_op jit(solution)/shard_map/ppermute | solution.py:110
  50.8 38.5 %collective-permute-start.8 = (bf16[512,1664]{1,0:T(8,128)(2,1)}, bf16[512,1664]{1,0:T(8,128)(2,1)}, u32[]{:S(2)}, u32[]{:S(2)}) collective-permute-start(bf16[512,1664]{1,0:T(8,128)(2,1)} %shard_map.145.refs_0_), channel_id=1, source_target_pairs={{0,4},{4,0},{8,12},{12,8},{16,20},{20,16},{24,28},{28,24},{32,36},... | collective-permute-start | bytes 5111816 | tf_op jit(solution)/shard_map/ppermute | solution.py:116
  59.0 22.9 %copy-start.11 = (f32[128]{0:T(128)S(1)}, f32[128]{0:T(128)}, u32[]{:S(2)}) copy-start(f32[128]{0:T(128)} %constant.45.clone) | copy-start | bytes 1540
  59.0 30.3 %copy-start.7 = (f32[3,256]{1,0:T(4,128)S(1)}, f32[3,256]{1,0:T(4,128)}, u32[]{:S(2)}) copy-start(f32[3,256]{1,0:T(4,128)} %refs_10_.1) | copy-start | bytes 9220
  59.0 30.3 %copy-start.8 = (f32[4]{0:T(128)S(1)}, f32[4]{0:T(128)}, u32[]{:S(2)}) copy-start(f32[4]{0:T(128)} %sink_ref.1) | copy-start | bytes 52
  59.0 30.3 %copy-start.9 = (f32[64]{0:T(128)S(1)}, f32[64]{0:T(128)}, u32[]{:S(2)}) copy-start(f32[64]{0:T(128)} %param.23) | copy-start | bytes 772
  59.0 30.3 %copy-start.10 = (f32[64]{0:T(128)S(1)}, f32[64]{0:T(128)}, u32[]{:S(2)}) copy-start(f32[64]{0:T(128)} %param.24) | copy-start | bytes 772
  59.0 30.3 %all-to-all-start = ((bf16[4,128,2048]{2,1,0:T(8,128)(2,1)}), bf16[4,128,2048]{2,1,0:T(8,128)(2,1)S(1)}, u32[]{:S(2)}, u32[]{:S(2)}) async-start(bf16[4,128,2048]{2,1,0:T(8,128)(2,1)} %rows.1), calls=%async_computation | async-start | bytes 4194304 | tf_op jit(solution)/shard_map/all_to_all | solution.py:153
  63.2 0.8 copy-start.5
  63.9 1.0 copy-start.4
  65.0 1.0 copy-start.6
  67.1 22.3 %collective-permute-start.9 = (bf16[384,1664]{1,0:T(8,128)(2,1)S(1)}, bf16[384,1664]{1,0:T(8,128)(2,1)}, u32[]{:S(2)}, u32[]{:S(2)}) collective-permute-start(bf16[384,1664]{1,0:T(8,128)(2,1)S(1)} %shard_map.146.refs_1_), channel_id=1, source_target_pairs={{0,4},{4,0},{8,12},{12,8},{16,20},{20,16},{24,28},{28,24},{32,36},... | collective-permute-start | bytes 3833864 | tf_op jit(solution)/shard_map/ppermute | solution.py:116
  69.3 10.6 %collective-permute-start.7 = (bf16[128,1664]{1,0:T(8,128)(2,1)}, bf16[128,1664]{1,0:T(8,128)(2,1)}, u32[]{:S(2)}, u32[]{:S(2)}) collective-permute-start(bf16[128,1664]{1,0:T(8,128)(2,1)} %collective-permute-done.5.refs_1_), channel_id=1, source_target_pairs={{0,56},{4,452},{8,16},{12,460},{16,8},{20,468},{24,32},{28,476},{3... | collective-permute-start | bytes 1277960 | tf_op jit(solution)/shard_map/ppermute | solution.py:112
  79.9 9.5 %collective-permute-start.10 = (bf16[128,1664]{1,0:T(8,128)(2,1)}, bf16[128,1664]{1,0:T(8,128)(2,1)}, u32[]{:S(2)}, u32[]{:S(2)}) collective-permute-start(bf16[128,1664]{1,0:T(8,128)(2,1)} %collective-permute-done.7.refs_2_), channel_id=1, source_target_pairs={{0,4},{4,0},{8,12},{12,8},{16,20},{20,16},{24,28},{28,24},{32,36},... | collective-permute-start | bytes 1277960 | tf_op jit(solution)/shard_map/ppermute | solution.py:116
  89.4 1.0 copy-start
  90.3 0.9 copy-start.1

commit v3 on v2

--- a/solution.py
+++ b/solution.py
@@ -161,8 +161,8 @@
     for first, second, third in (refs[:3], refs[3:6]):
         pieces += [(first, k * 128) for k in range(4)]
         pieces += [(second, k * 128) for k in range(3)] + [(third, 0)]
-    cos_ref, sin_ref, qg_ref, kg_ref, conv_ref, out_ref = refs[6:12]
-    w_s, p_s, kk_s, vv_s, prod_s, act_s = refs[12:]
+    turn_ref, qg_ref, kg_ref, conv_ref, out_ref = refs[6:11]
+    w_s, p_s, kv_s, kk_s, vv_s, prod_s, act_s = refs[11:]
     core, y, z, place = where_ref[0], where_ref[1], where_ref[2], where_ref[3]
 
     for k, (piece, base) in enumerate(pieces):
@@ -177,17 +177,19 @@
             ]
 
     features = x_ref.shape[-1]
-    main = x_ref[:, :LOCAL, :].reshape(MAIN, features)
-    rim = x_ref[:, LOCAL:, :].reshape(MAIN, features)
-    for lo in range(0, PROJ, 128):
-        cols = slice(lo, lo + 128)
-        part = jnp.dot(main, w_s[:, cols], preferred_element_type=jnp.float32)
-        p_s[WINDOW : WINDOW + MAIN, cols] = part.astype(jnp.bfloat16)
-        if lo < 256 or 384 <= lo < 640:
-            continue
-        part = jnp.dot(rim, w_s[:, cols], preferred_element_type=jnp.float32).astype(jnp.bfloat16)
-        p_s[:WINDOW, cols] = part[WINDOW:]
-        p_s[WINDOW + MAIN :, cols] = part[:WINDOW]
+    raw = x_ref[...].reshape(ROWS, features)
+    pairs = jnp.dot(raw, w_s[:, 256:384], preferred_element_type=jnp.float32).astype(jnp.bfloat16)
+    for x in range(TP):
+        base = x * SHARE
+        kv_s[WINDOW + x * LOCAL : WINDOW + (x + 1) * LOCAL, :] = pairs[base : base + LOCAL]
+        to = (x - 2) * LOCAL if x >= 2 else WINDOW + MAIN + x * LOCAL
+        kv_s[to : to + LOCAL, :] = pairs[base + LOCAL : base + SHARE]
+
+    edges = [x_ref[TP - 1, SHARE - 8 :, :], x_ref[0, LOCAL : LOCAL + 8, :]]
+    main = jnp.concatenate([x_ref[:, :LOCAL, :].reshape(MAIN, features)] + edges, axis=0)
+    for lo in (0, 384, 640, 896):
+        part = jnp.dot(main, w_s[:, lo : lo + 256], preferred_element_type=jnp.float32)
+        p_s[:, lo : lo + 256] = part.astype(jnp.bfloat16)
 
     def gain_rows(ref, scale):
         gain = jnp.concatenate([ref[...], ref[...]], axis=1) * scale
@@ -210,12 +212,15 @@
             pltpu.roll(scaled, 2 * HEAD - HALF, 1),
             pltpu.roll(scaled, HALF, 1),
         )
-        cosine = cos_ref[at : at + BLOCK, :]
-        sine = sin_ref[at : at + BLOCK, :]
+        row = BLOCK + at // BLOCK
+        cos0, sin0 = turn_ref[0, row : row + 1, :], turn_ref[1, row : row + 1, :]
+        cos1, sin1 = turn_ref[0, :BLOCK, :], turn_ref[1, :BLOCK, :]
+        cosine = cos0 * cos1 - sin0 * sin1
+        sine = sin0 * cos1 + cos0 * sin1
         return scaled * (cosine * gain) + crossed * (sine * crossed_gain)
 
     for at in range(0, ROWS, BLOCK):
-        kv = p_s[at : at + BLOCK, 256:384].astype(jnp.float32)
+        kv = kv_s[at : at + BLOCK, :].astype(jnp.float32)
         lane = lax.broadcasted_iota(jnp.int32, kv.shape, 1)
         key = rotated(kv, at, *key_gain)
         kk_s[at : at + BLOCK, :] = jnp.where(lane < HEAD, key, pltpu.roll(key, HEAD, 1)).astype(
@@ -224,17 +229,15 @@
         vv_s[at : at + BLOCK, :] = jnp.where(lane < HEAD, pltpu.roll(kv, HEAD, 1), kv).astype(
             jnp.bfloat16
         )
-        prod_s[at : at + BLOCK, :] = (
-            (
-                p_s[at : at + BLOCK, 640:896].astype(jnp.float32)
-                * p_s[at : at + BLOCK, 896:1152].astype(jnp.float32)
-            )
-            .astype(jnp.bfloat16)
-            .astype(jnp.float32)
-        )
+
+    product = p_s[:, 640:896].astype(jnp.float32) * p_s[:, 896:1152].astype(jnp.float32)
+    product = product.astype(jnp.bfloat16).astype(jnp.float32)
+    prod_s[8 : 8 + MAIN, :] = product[:MAIN]
+    prod_s[:8, :] = product[MAIN : MAIN + 8]
+    prod_s[8 + MAIN :, :] = product[MAIN + 8 :]
 
     for at in range(0, MAIN, BLOCK):
-        rows = slice(at + WINDOW, at + WINDOW + BLOCK)
+        rows = slice(at, at + BLOCK)
         keys = kk_s[at : at + 3 * BLOCK, :]
         values = vv_s[at : at + 3 * BLOCK, :]
         shape = (BLOCK, 3 * BLOCK)
@@ -242,31 +245,38 @@
         k_at = lax.broadcasted_iota(jnp.int32, shape, 1) - WINDOW
         k_pos = k_at + (place * MAIN + at)
         allowed = (jnp.abs(q_at - k_at) <= WINDOW) & (k_pos >= 0) & (k_pos < SP * MAIN)
+        low = lax.broadcasted_iota(jnp.int32, (BLOCK, 128), 1) < HEAD
+        queries = []
         for pair in range(2):
             lanes = slice(pair * 128, (pair + 1) * 128)
             query = rotated(p_s[rows, lanes].astype(jnp.float32), at + WINDOW, *query_gain)
-            low = lax.broadcasted_iota(jnp.int32, query.shape, 1) < HEAD
-            outs = []
-            for head in range(2):
-                q_head = jnp.where(low if head == 0 else ~low, query, 0.0).astype(jnp.bfloat16)
-                scores = lax.dot_general(
-                    q_head, keys, (((1,), (1,)), ((), ())), preferred_element_type=jnp.float32
-                )
-                scores = jnp.where(allowed, scores, NEG_FILL)
-                sink = sink_ref[2 * pair + head]
-                top = jnp.maximum(jnp.max(scores, axis=-1, keepdims=True), sink)
-                expo = jnp.exp(scores - top)
-                total = jnp.sum(expo, axis=-1, keepdims=True) + jnp.exp(sink - top)
-                weights = (expo * (1.0 / total)).astype(jnp.bfloat16)
-                outs.append(jnp.dot(weights, values, preferred_element_type=jnp.float32))
-            act_s[at : at + BLOCK, lanes] = jnp.where(low, outs[0], outs[1]).astype(jnp.bfloat16)
-        lo = at + WINDOW
+            queries += [jnp.where(low, query, 0.0), jnp.where(low, 0.0, query)]
+        stacked = jnp.concatenate(queries, axis=0).astype(jnp.bfloat16)
+        scores = lax.dot_general(
+            stacked, keys, (((1,), (1,)), ((), ())), preferred_element_type=jnp.float32
+        )
+        weights = []
+        for head in range(4):
+            score = jnp.where(allowed, scores[head * BLOCK : (head + 1) * BLOCK], NEG_FILL)
+            sink = sink_ref[head]
+            top = jnp.maximum(jnp.max(score, axis=-1, keepdims=True), sink)
+            expo = jnp.exp(score - top)
+            total = jnp.sum(expo, axis=-1, keepdims=True) + jnp.exp(sink - top)
+            weights.append((expo * (1.0 / total)).astype(jnp.bfloat16))
+        outs = jnp.dot(
+            jnp.concatenate(weights, axis=0), values, preferred_element_type=jnp.float32
+        ).astype(jnp.bfloat16)
+        for pair in range(2):
+            first = outs[2 * pair * BLOCK : (2 * pair + 1) * BLOCK]
+            second = outs[(2 * pair + 1) * BLOCK : (2 * pair + 2) * BLOCK]
+            act_s[rows, pair * 128 : (pair + 1) * 128] = jnp.where(low, first, second)
+        lo = at + 8
         mixed = (
             conv_ref[0:1, :] * prod_s[lo - 1 : lo - 1 + BLOCK, :]
             + conv_ref[1:2, :] * prod_s[lo : lo + BLOCK, :]
             + conv_ref[2:3, :] * prod_s[lo + 1 : lo + 1 + BLOCK, :]
         )
-        act_s[at : at + BLOCK, 256:512] = (p_s[rows, 384:640].astype(jnp.float32) * mixed).astype(
+        act_s[rows, 256:512] = (p_s[rows, 384:640].astype(jnp.float32) * mixed).astype(
             jnp.bfloat16
         )
 
@@ -288,10 +298,11 @@
         out_specs=VMEM,
         scratch_shapes=[
             pltpu.VMEM((features, WIDTH), jnp.bfloat16),
-            pltpu.VMEM((ROWS, PROJ), jnp.bfloat16),
+            pltpu.VMEM((MAIN + 16, PROJ), jnp.bfloat16),
             pltpu.VMEM((ROWS, 128), jnp.bfloat16),
             pltpu.VMEM((ROWS, 128), jnp.bfloat16),
-            pltpu.VMEM((ROWS, 256), jnp.float32),
+            pltpu.VMEM((ROWS, 128), jnp.bfloat16),
+            pltpu.VMEM((MAIN + 16, 256), jnp.float32),
             pltpu.VMEM((MAIN, 512), jnp.bfloat16),
         ],
         compiler_params=pltpu.CompilerParams(vmem_limit_bytes=32 * MIB),
@@ -330,9 +341,11 @@
             out_conv,
         )
     )
-    positions = (place * MAIN - WINDOW + jnp.arange(ROWS, dtype=jnp.int32)).astype(jnp.float32)
-    angle = positions[:, None] * ANGLES
-    tables = (jnp.cos(angle), jnp.sin(angle), query_gain[None], key_gain[None])
+    starts = place * MAIN - WINDOW + BLOCK * jnp.arange(8, dtype=jnp.int32)
+    rows = jnp.concatenate([jnp.arange(BLOCK, dtype=jnp.int32), starts]).astype(jnp.float32)
+    angle = rows[:, None] * ANGLES
+    turns = jnp.stack([jnp.cos(angle), jnp.sin(angle)])
+    tables = (turns, query_gain[None], key_gain[None])
     partial = run_layer(where, sink_logit, gathered, pieces, tables, conv_weight)
     blocks = lax.all_to_all(partial.reshape(TP, LOCAL, -1), "tp", 0, 0, tiled=True)
     return blocks.astype(jnp.float32).sum(axis=0).astype(jnp.bfloat16)

time: 122 us -> 116 us (0.951)
  Pallas kernels: 18 us -> 14.3 us
  local copies, waits for them, and re-layouts: 4.7 us -> 2.82 us
  other arithmetic: 2.8 us -> 1.35 us
  waiting for transfers between devices: 19.1 us -> 20.5 us
    pallas_call x1, Pallas kernels: 10.7 us -> 6.98 us  [run_layer(): pl.pallas_call(layer_kernel, out_shape=jax.ShapeDtypeStruct((MAIN, featur...]
    unnamed x24 -> x20, local copies, waits for them, and re-layouts: 4.7 us -> 2.82 us
    sin x1 -> x0, other arithmetic: 1.8 us -> none  [per_device(): tables = (jnp.cos(angle), jnp.sin(angle), query_gain[None], key_gain[None])]
    all_to_all x1, waiting for transfers between devices: 5.65 us -> 7.09 us  [gathered_tokens(): return lax.all_to_all(sent, 'tp', 0, 0, tiled=True)]
  transfers between devices with their start and end apart: 12 -> 12, of which waited for: 4 -> 4; matrix products, arithmetic and copies ran while one was open for 2% -> 0% of each run, Pallas kernels for 5% -> 5%
where the time goes in v3:
time: 116 us; the launch traced here: 114 us
  starting transfers between devices  42.9 us (37%)
  blocking collectives  31.6 us (27%)
  waiting for transfers between devices  20.5 us (18%)
  Pallas kernels  14.3 us (12%)
  local copies, waits for them, and re-layouts  2.82 us (2%)
  other arithmetic  1.35 us (1%)
    all_to_all x1, blocking collectives, per_device(): lax.all_to_all(partial.reshape(TP, LOCAL, -1), 'tp', 0, 0, tiled=True)  16.5 us
    all_to_all x1, blocking collectives, gathered_weights(): lax.all_to_all(blocks, 'sp', 0, 0, axis_index_groups=GROUPS, tiled=True)  15.2 us
    ppermute x3, starting transfers between devices, gathered_weights(): return kept + tuple((lax.ppermute(p, 'sp', SWAP) for p in kept))  10.8 us
    ppermute x1, starting transfers between devices, gathered_weights(): o1 = lax.ppermute(own, 'sp', ODD)  10.7 us
    ppermute x1, waiting for transfers between devices, gathered_weights(): o4 = lax.ppermute(e3, 'sp', ODD)  8.09 us
    all_to_all x1, waiting for transfers between devices, gathered_tokens(): return lax.all_to_all(sent, 'tp', 0, 0, tiled=True)  7.09 us
    pallas_call x1, Pallas kernels, run_layer(): pl.pallas_call(layer_kernel, out_shape=jax.ShapeDtypeStruct((MAIN, featur...  6.98 us
    all_to_all x1, starting transfers between devices, gathered_tokens(): return lax.all_to_all(sent, 'tp', 0, 0, tiled=True)  4.16 us
  transfers between devices with their start and end apart: 12, of which 4 were waited for; matrix products, arithmetic and copies ran while one was open for 0% of the time, Pallas kernels for 5%

profile of v3, /device:TPU:17, one launch (start us, length us, event | category | flops | bytes accessed | tf_op | source)
XLA Modules:
  0.0 113.7 jit_solution(18097827124601369919)
XLA Ops:
  0.0 1.7 %copies.1 = bf16[8,16,1664]{2,1,0:T(8,128)(2,1)} custom-call(bf16[16,256]{1,0:T(8,128)(2,1)} %bitcast.23, bf16[16,64]{1,0:T(8,128)(2,1)} %bitcast.30, bf16[16,64]{1,0:T(8,128)(2,1)} %bitcast.31, bf16[16,256]{1,0:T(8,128)(2,1)} %bitcast.24, bf16[16,256]{1,0:T(8,128)(2,1)} %bitcast.25, bf16[16,256]{1,0:T(8,128)(2,1)} %bitcast.26, bf16[16,256]{1,0:T(8,128)(2,1)} %bitcast.27, ...), custom_call_target="tpu_custom_call" | custom-call | tf_op jit(solution)/shard_map/copies/pallas_call | solution.py:76
  1.7 15.2 %all_to_all.15 = bf16[8,16,1664]{2,1,0:T(8,128)(2,1)S(1)} all-to-all(bf16[8,16,1664]{2,1,0:T(8,128)(2,1)} %copies.1), channel_id=1, replica_groups={{0,64,128,192,256,320,384,448},{8,72,136,200,264,328,392,456},{16,80,14..., dimensions={0} | all-to-all | bytes 851968 | tf_op jit(solution)/shard_map/all_to_all | solution.py:104
  16.8 10.7 %collective-permute-start.2 = (bf16[128,1664]{1,0:T(8,128)(2,1)S(1)}, bf16[128,1664]{1,0:T(8,128)(2,1)S(1)}, u32[]{:S(2)}, u32[]{:S(2)}) collective-permute-start(bf16[128,1664]{1,0:T(8,128)(2,1)S(1)} %bitcast.18), channel_id=1, source_target_pairs={{0,56},{4,452},{8,16},{12,460},{16,8},{20,468},{24,32},{28,476},{3... | collective-permute-start | bytes 1277960 | tf_op jit(solution)/shard_map/ppermute | solution.py:107
  27.5 1.9 %collective-permute-start.1 = (bf16[128,1664]{1,0:T(8,128)(2,1)S(1)}, bf16[128,1664]{1,0:T(8,128)(2,1)S(1)}, u32[]{:S(2)}, u32[]{:S(2)}) collective-permute-start(bf16[128,1664]{1,0:T(8,128)(2,1)S(1)} %bitcast.19), channel_id=1, source_target_pairs={{0,8},{4,68},{8,0},{12,76},{16,24},{20,84},{24,16},{28,92},{32,40}... | collective-permute-start | bytes 1277960 | tf_op jit(solution)/shard_map/ppermute | solution.py:106
  29.4 3.6 %collective-permute-done.2.refs_2_ = bf16[128,1664]{1,0:T(8,128)(2,1)S(1)} collective-permute-done((bf16[128,1664]{1,0:T(8,128)(2,1)S(1)}, bf16[128,1664]{1,0:T(8,128)(2,1)S(1)}, u32[]{:S(2)}, u32[]{:S(2)}) %collective-permute-start.2) | collective-permute-done | bytes 426016 | tf_op jit(solution)/shard_map/ppermute | solution.py:107
  33.0 1.9 %collective-permute-start.4 = (bf16[128,1664]{1,0:T(8,128)(2,1)S(1)}, bf16[128,1664]{1,0:T(8,128)(2,1)S(1)}, u32[]{:S(2)}, u32[]{:S(2)}) collective-permute-start(bf16[128,1664]{1,0:T(8,128)(2,1)S(1)} %collective-permute-done.2.refs_2_), channel_id=1, source_target_pairs={{0,8},{4,68},{8,0},{12,76},{16,24},{20,84},{24,16},{28,92},{32,40}... | collective-permute-start | bytes 1277960 | tf_op jit(solution)/shard_map/ppermute | solution.py:109
  34.9 1.7 %collective-permute-done.1.refs_1_ = bf16[128,1664]{1,0:T(8,128)(2,1)S(1)} collective-permute-done((bf16[128,1664]{1,0:T(8,128)(2,1)S(1)}, bf16[128,1664]{1,0:T(8,128)(2,1)S(1)}, u32[]{:S(2)}, u32[]{:S(2)}) %collective-permute-start.1) | collective-permute-done | bytes 426016 | tf_op jit(solution)/shard_map/ppermute | solution.py:106
  36.6 2.8 %collective-permute-start.3 = (bf16[128,1664]{1,0:T(8,128)(2,1)S(1)}, bf16[128,1664]{1,0:T(8,128)(2,1)S(1)}, u32[]{:S(2)}, u32[]{:S(2)}) collective-permute-start(bf16[128,1664]{1,0:T(8,128)(2,1)S(1)} %collective-permute-done.1.refs_1_), channel_id=1, source_target_pairs={{0,56},{4,452},{8,16},{12,460},{16,8},{20,468},{24,32},{28,476},{3... | collective-permute-start | bytes 1277960 | tf_op jit(solution)/shard_map/ppermute | solution.py:108
  39.5 1.8 %norm.1.normed = bf16[64,2048]{1,0:T(8,128)(2,1)} custom-call(bf16[64,2048]{1,0:T(8,128)(2,1)} %x_ref.1, f32[1,2048]{1,0:T(1,128)} %bitcast.29), custom_call_target="tpu_custom_call" | custom-call | tf_op jit(solution)/shard_map/norm/pallas_call | solution.py:141
  41.3 4.1 %collective-permute-start = (bf16[64,2048]{1,0:T(8,128)(2,1)}, bf16[64,2048]{1,0:T(8,128)(2,1)S(1)}, u32[]{:S(2)}, u32[]{:S(2)}) collective-permute-start(bf16[64,2048]{1,0:T(8,128)(2,1)} %norm.1.normed), channel_id=1, source_target_pairs={{2,6},{3,7},{6,10},{7,11},{10,14},{11,15},{14,18},{15,19},{18,22},... | collective-permute-start | bytes 786440 | tf_op jit(solution)/shard_map/ppermute | solution.py:151
  45.4 1.9 %collective-permute-start.6 = (bf16[128,1664]{1,0:T(8,128)(2,1)S(1)}, bf16[128,1664]{1,0:T(8,128)(2,1)S(1)}, u32[]{:S(2)}, u32[]{:S(2)}) collective-permute-start(bf16[128,1664]{1,0:T(8,128)(2,1)S(1)} %collective-permute-done.4.refs_0_), channel_id=1, source_target_pairs={{0,56},{4,452},{8,16},{12,460},{16,8},{20,468},{24,32},{28,476},{3... | collective-permute-start | bytes 1277960 | tf_op jit(solution)/shard_map/ppermute | solution.py:111
  47.3 2.2 %collective-permute-start.5 = (bf16[128,1664]{1,0:T(8,128)(2,1)S(1)}, bf16[128,1664]{1,0:T(8,128)(2,1)}, u32[]{:S(2)}, u32[]{:S(2)}) collective-permute-start(bf16[128,1664]{1,0:T(8,128)(2,1)S(1)} %collective-permute-done.3.refs_3_), channel_id=1, source_target_pairs={{0,8},{4,68},{8,0},{12,76},{16,24},{20,84},{24,16},{28,92},{32,40}... | collective-permute-start | bytes 1277960 | tf_op jit(solution)/shard_map/ppermute | solution.py:110
  49.5 1.3 %shard_map.145.refs_0_ = bf16[512,1664]{1,0:T(8,128)(2,1)} custom-call(bf16[128,1664]{1,0:T(8,128)(2,1)S(1)} %bitcast.20, bf16[128,1664]{1,0:T(8,128)(2,1)S(1)} %collective-permute-done.1.refs_1_, bf16[128,1664]{1,0:T(8,128)(2,1)S(1)} %collective-permute-done.2.refs_2_, bf16[128,1664]{1,0:T(8,128)(2,1)S(1)} %collective-permute-done.3.refs_3_), custom_call_target="tpu_custom_call" | custom-call | tf_op jit(solution)/shard_map/pallas_call | solution.py:125
  50.8 6.7 %collective-permute-start.8 = (bf16[512,1664]{1,0:T(8,128)(2,1)}, bf16[512,1664]{1,0:T(8,128)(2,1)}, u32[]{:S(2)}, u32[]{:S(2)}) collective-permute-start(bf16[512,1664]{1,0:T(8,128)(2,1)} %shard_map.145.refs_0_), channel_id=1, source_target_pairs={{0,4},{4,0},{8,12},{12,8},{16,20},{20,16},{24,28},{28,24},{32,36},... | collective-permute-start | bytes 5111816 | tf_op jit(solution)/shard_map/ppermute | solution.py:116
  57.5 1.5 %rows.1 = bf16[4,128,2048]{2,1,0:T(8,128)(2,1)} custom-call(bf16[64,2048]{1,0:T(8,128)(2,1)S(1)} %copy-done, bf16[64,2048]{1,0:T(8,128)(2,1)S(1)} %collective-permute-done.rim), custom_call_target="tpu_custom_call" | custom-call | tf_op jit(solution)/shard_map/rows/pallas_call | solution.py:92
  59.0 4.2 %all-to-all-start = ((bf16[4,128,2048]{2,1,0:T(8,128)(2,1)}), bf16[4,128,2048]{2,1,0:T(8,128)(2,1)S(1)}, u32[]{:S(2)}, u32[]{:S(2)}) async-start(bf16[4,128,2048]{2,1,0:T(8,128)(2,1)} %rows.1), calls=%async_computation | async-start | bytes 4194304 | tf_op jit(solution)/shard_map/all_to_all | solution.py:153
  66.0 1.1 shard_map.146.refs_1_
  67.1 2.2 %collective-permute-start.9 = (bf16[384,1664]{1,0:T(8,128)(2,1)S(1)}, bf16[384,1664]{1,0:T(8,128)(2,1)}, u32[]{:S(2)}, u32[]{:S(2)}) collective-permute-start(bf16[384,1664]{1,0:T(8,128)(2,1)S(1)} %shard_map.146.refs_1_), channel_id=1, source_target_pairs={{0,4},{4,0},{8,12},{12,8},{16,20},{20,16},{24,28},{28,24},{32,36},... | collective-permute-start | bytes 3833864 | tf_op jit(solution)/shard_map/ppermute | solution.py:116
  69.3 2.4 %collective-permute-start.7 = (bf16[128,1664]{1,0:T(8,128)(2,1)}, bf16[128,1664]{1,0:T(8,128)(2,1)}, u32[]{:S(2)}, u32[]{:S(2)}) collective-permute-start(bf16[128,1664]{1,0:T(8,128)(2,1)} %collective-permute-done.5.refs_1_), channel_id=1, source_target_pairs={{0,56},{4,452},{8,16},{12,460},{16,8},{20,468},{24,32},{28,476},{3... | collective-permute-start | bytes 1277960 | tf_op jit(solution)/shard_map/ppermute | solution.py:112
  71.8 8.1 %collective-permute-done.7.refs_2_ = bf16[128,1664]{1,0:T(8,128)(2,1)} collective-permute-done((bf16[128,1664]{1,0:T(8,128)(2,1)}, bf16[128,1664]{1,0:T(8,128)(2,1)}, u32[]{:S(2)}, u32[]{:S(2)}) %collective-permute-start.7) | collective-permute-done | bytes 426016 | tf_op jit(solution)/shard_map/ppermute | solution.py:112
  79.9 1.9 %collective-permute-start.10 = (bf16[128,1664]{1,0:T(8,128)(2,1)}, bf16[128,1664]{1,0:T(8,128)(2,1)}, u32[]{:S(2)}, u32[]{:S(2)}) collective-permute-start(bf16[128,1664]{1,0:T(8,128)(2,1)} %collective-permute-done.7.refs_2_), channel_id=1, source_target_pairs={{0,4},{4,0},{8,12},{12,8},{16,20},{20,16},{24,28},{28,24},{32,36},... | collective-permute-start | bytes 1277960 | tf_op jit(solution)/shard_map/ppermute | solution.py:116
  82.2 7.1 %all-to-all-done.x_ref = bf16[4,128,2048]{2,1,0:T(8,128)(2,1)S(1)} async-done(((bf16[4,128,2048]{2,1,0:T(8,128)(2,1)}), bf16[4,128,2048]{2,1,0:T(8,128)(2,1)S(1)}, u32[]{:S(2)}, u32[]{:S(2)}) %all-to-all-start) | async-done | bytes 2097184 | tf_op jit(solution)/shard_map/all_to_all | solution.py:153
  89.4 7.0 %layer.1 = bf16[256,2048]{1,0:T(8,128)(2,1)S(1)} custom-call(s32[4]{0:T(128)S(1)} %pad_add_fusion.where_ref, f32[4]{0:T(128)S(1)} %copy-done.6, bf16[4,128,2048]{2,1,0:T(8,128)(2,1)S(1)} %all-to-all-done.x_ref, bf16[512,1664]{1,0:T(8,128)(2,1)} %shard_map.145.refs_0_, bf16[384,1664]{1,0:T(8,128)(2,1)S(1)} %shard_map.146.refs_1_, ...), custom_call_target="tpu_custom_call" | custom-call | tf_op jit(solution)/shard_map/layer/pallas_call | solution.py:294
  96.4 16.5 %all_to_all.16 = bf16[4,64,2048]{2,1,0:T(8,128)(2,1)S(1)} all-to-all(bf16[4,64,2048]{2,1,0:T(8,128)(2,1)S(1)} %bitcast.17), channel_id=1, replica_groups=mesh['sp'=128,'tp'=4] {'tp'}, dimensions={0} | all-to-all | bytes 2097152 | tf_op jit(solution)/shard_map/all_to_all | solution.py:350
  (35 shorter events, 4.2 us)
Async XLA Ops:
  16.8 16.2 %collective-permute-start.2 = (bf16[128,1664]{1,0:T(8,128)(2,1)S(1)}, bf16[128,1664]{1,0:T(8,128)(2,1)S(1)}, u32[]{:S(2)}, u32[]{:S(2)}) collective-permute-start(bf16[128,1664]{1,0:T(8,128)(2,1)S(1)} %bitcast.18), channel_id=1, source_target_pairs={{0,56},{4,452},{8,16},{12,460},{16,8},{20,468},{24,32},{28,476},{3... | collective-permute-start | bytes 1277960 | tf_op jit(solution)/shard_map/ppermute | solution.py:107
  27.5 9.2 %collective-permute-start.1 = (bf16[128,1664]{1,0:T(8,128)(2,1)S(1)}, bf16[128,1664]{1,0:T(8,128)(2,1)S(1)}, u32[]{:S(2)}, u32[]{:S(2)}) collective-permute-start(bf16[128,1664]{1,0:T(8,128)(2,1)S(1)} %bitcast.19), channel_id=1, source_target_pairs={{0,8},{4,68},{8,0},{12,76},{16,24},{20,84},{24,16},{28,92},{32,40}... | collective-permute-start | bytes 1277960 | tf_op jit(solution)/shard_map/ppermute | solution.py:106
  33.0 12.4 %collective-permute-start.4 = (bf16[128,1664]{1,0:T(8,128)(2,1)S(1)}, bf16[128,1664]{1,0:T(8,128)(2,1)S(1)}, u32[]{:S(2)}, u32[]{:S(2)}) collective-permute-start(bf16[128,1664]{1,0:T(8,128)(2,1)S(1)} %collective-permute-done.2.refs_2_), channel_id=1, source_target_pairs={{0,8},{4,68},{8,0},{12,76},{16,24},{20,84},{24,16},{28,92},{32,40}... | collective-permute-start | bytes 1277960 | tf_op jit(solution)/shard_map/ppermute | solution.py:109
  36.6 10.7 %collective-permute-start.3 = (bf16[128,1664]{1,0:T(8,128)(2,1)S(1)}, bf16[128,1664]{1,0:T(8,128)(2,1)S(1)}, u32[]{:S(2)}, u32[]{:S(2)}) collective-permute-start(bf16[128,1664]{1,0:T(8,128)(2,1)S(1)} %collective-permute-done.1.refs_1_), channel_id=1, source_target_pairs={{0,56},{4,452},{8,16},{12,460},{16,8},{20,468},{24,32},{28,476},{3... | collective-permute-start | bytes 1277960 | tf_op jit(solution)/shard_map/ppermute | solution.py:108
  41.3 16.2 %copy-start = (bf16[64,2048]{1,0:T(8,128)(2,1)S(1)}, bf16[64,2048]{1,0:T(8,128)(2,1)}, u32[]{:S(2)}) copy-start(bf16[64,2048]{1,0:T(8,128)(2,1)} %norm.1.normed) | copy-start | bytes 786436
  41.3 16.2 %collective-permute-start = (bf16[64,2048]{1,0:T(8,128)(2,1)}, bf16[64,2048]{1,0:T(8,128)(2,1)S(1)}, u32[]{:S(2)}, u32[]{:S(2)}) collective-permute-start(bf16[64,2048]{1,0:T(8,128)(2,1)} %norm.1.normed), channel_id=1, source_target_pairs={{2,6},{3,7},{6,10},{7,11},{10,14},{11,15},{14,18},{15,19},{18,22},... | collective-permute-start | bytes 786440 | tf_op jit(solution)/shard_map/ppermute | solution.py:151
  45.4 5.5 %copy-start.1 = (bf16[128,1664]{1,0:T(8,128)(2,1)}, bf16[128,1664]{1,0:T(8,128)(2,1)S(1)}, u32[]{:S(2)}) copy-start(bf16[128,1664]{1,0:T(8,128)(2,1)S(1)} %collective-permute-done.4.refs_0_) | copy-start | bytes 1277956
  45.4 17.8 %collective-permute-start.6 = (bf16[128,1664]{1,0:T(8,128)(2,1)S(1)}, bf16[128,1664]{1,0:T(8,128)(2,1)S(1)}, u32[]{:S(2)}, u32[]{:S(2)}) collective-permute-start(bf16[128,1664]{1,0:T(8,128)(2,1)S(1)} %collective-permute-done.4.refs_0_), channel_id=1, source_target_pairs={{0,56},{4,452},{8,16},{12,460},{16,8},{20,468},{24,32},{28,476},{3... | collective-permute-start | bytes 1277960 | tf_op jit(solution)/shard_map/ppermute | solution.py:111
  47.3 16.6 %collective-permute-start.5 = (bf16[128,1664]{1,0:T(8,128)(2,1)S(1)}, bf16[128,1664]{1,0:T(8,128)(2,1)}, u32[]{:S(2)}, u32[]{:S(2)}) collective-permute-start(bf16[128,1664]{1,0:T(8,128)(2,1)S(1)} %collective-permute-done.3.refs_3_), channel_id=1, source_target_pairs={{0,8},{4,68},{8,0},{12,76},{16,24},{20,84},{24,16},{28,92},{32,40}... | collective-permute-start | bytes 1277960 | tf_op jit(solution)/shard_map/ppermute | solution.py:110
  50.8 38.5 %collective-permute-start.8 = (bf16[512,1664]{1,0:T(8,128)(2,1)}, bf16[512,1664]{1,0:T(8,128)(2,1)}, u32[]{:S(2)}, u32[]{:S(2)}) collective-permute-start(bf16[512,1664]{1,0:T(8,128)(2,1)} %shard_map.145.refs_0_), channel_id=1, source_target_pairs={{0,4},{4,0},{8,12},{12,8},{16,20},{20,16},{24,28},{28,24},{32,36},... | collective-permute-start | bytes 5111816 | tf_op jit(solution)/shard_map/ppermute | solution.py:116
  59.0 22.9 %copy-start.9 = (f32[128]{0:T(128)S(1)}, f32[128]{0:T(128)}, u32[]{:S(2)}) copy-start(f32[128]{0:T(128)} %constant.47.clone) | copy-start | bytes 1540
  59.0 30.3 %copy-start.5 = (f32[3,256]{1,0:T(4,128)S(1)}, f32[3,256]{1,0:T(4,128)}, u32[]{:S(2)}) copy-start(f32[3,256]{1,0:T(4,128)} %refs_9_.1) | copy-start | bytes 9220
  59.0 30.3 %copy-start.6 = (f32[4]{0:T(128)S(1)}, f32[4]{0:T(128)}, u32[]{:S(2)}) copy-start(f32[4]{0:T(128)} %sink_ref.1) | copy-start | bytes 52
  59.0 30.3 %copy-start.7 = (f32[64]{0:T(128)S(1)}, f32[64]{0:T(128)}, u32[]{:S(2)}) copy-start(f32[64]{0:T(128)} %param.23) | copy-start | bytes 772
  59.0 30.3 %copy-start.8 = (f32[64]{0:T(128)S(1)}, f32[64]{0:T(128)}, u32[]{:S(2)}) copy-start(f32[64]{0:T(128)} %param.24) | copy-start | bytes 772
  59.0 30.3 %all-to-all-start = ((bf16[4,128,2048]{2,1,0:T(8,128)(2,1)}), bf16[4,128,2048]{2,1,0:T(8,128)(2,1)S(1)}, u32[]{:S(2)}, u32[]{:S(2)}) async-start(bf16[4,128,2048]{2,1,0:T(8,128)(2,1)} %rows.1), calls=%async_computation | async-start | bytes 4194304 | tf_op jit(solution)/shard_map/all_to_all | solution.py:153
  63.2 0.8 copy-start.3
  64.0 1.0 copy-start.2
  65.0 1.0 copy-start.4
  67.1 22.2 %collective-permute-start.9 = (bf16[384,1664]{1,0:T(8,128)(2,1)S(1)}, bf16[384,1664]{1,0:T(8,128)(2,1)}, u32[]{:S(2)}, u32[]{:S(2)}) collective-permute-start(bf16[384,1664]{1,0:T(8,128)(2,1)S(1)} %shard_map.146.refs_1_), channel_id=1, source_target_pairs={{0,4},{4,0},{8,12},{12,8},{16,20},{20,16},{24,28},{28,24},{32,36},... | collective-permute-start | bytes 3833864 | tf_op jit(solution)/shard_map/ppermute | solution.py:116
  69.3 10.6 %collective-permute-start.7 = (bf16[128,1664]{1,0:T(8,128)(2,1)}, bf16[128,1664]{1,0:T(8,128)(2,1)}, u32[]{:S(2)}, u32[]{:S(2)}) collective-permute-start(bf16[128,1664]{1,0:T(8,128)(2,1)} %collective-permute-done.5.refs_1_), channel_id=1, source_target_pairs={{0,56},{4,452},{8,16},{12,460},{16,8},{20,468},{24,32},{28,476},{3... | collective-permute-start | bytes 1277960 | tf_op jit(solution)/shard_map/ppermute | solution.py:112
  79.9 9.4 %collective-permute-start.10 = (bf16[128,1664]{1,0:T(8,128)(2,1)}, bf16[128,1664]{1,0:T(8,128)(2,1)}, u32[]{:S(2)}, u32[]{:S(2)}) collective-permute-start(bf16[128,1664]{1,0:T(8,128)(2,1)} %collective-permute-done.7.refs_2_), channel_id=1, source_target_pairs={{0,4},{4,0},{8,12},{12,8},{16,20},{20,16},{24,28},{28,24},{32,36},... | collective-permute-start | bytes 1277960 | tf_op jit(solution)/shard_map/ppermute | solution.py:116

commit v4 on v3

--- a/solution.py
+++ b/solution.py
@@ -47,8 +47,13 @@
     return pairs
 
 
+def two_away(pos):
+    return (pos + 2) % RING if pos % 2 == 0 else (pos - 2) % RING
+
+
 EVEN = matching(even_partner)
 ODD = matching(odd_partner)
+FAR = matching(two_away)
 SWAP = [(2 * k + c, 2 * k + 1 - c) for k in range(CHIPS) for c in range(2)]
 GROUPS = [[sp_of(z, y, 0) for z in range(RING)] for y in range(RING)] + [
     [sp_of(z, y, 1) for y in range(RING)] for z in range(RING)
@@ -109,10 +114,10 @@
     e2 = lax.ppermute(o1, "sp", EVEN)
     e3 = lax.ppermute(o2, "sp", EVEN)
     o3 = lax.ppermute(e2, "sp", ODD)
-    o4 = lax.ppermute(e3, "sp", ODD)
+    f4 = lax.ppermute(o2, "sp", FAR)
     first = packed((own, e1, o1, o2))
-    second = packed((e2, e3, o3))
-    kept = (first, second, o4)
+    second = packed((e2, e3))
+    kept = (first, second, f4, o3)
     return kept + tuple(lax.ppermute(p, "sp", SWAP) for p in kept)
 
 
@@ -153,16 +158,16 @@
     return lax.all_to_all(sent, "tp", 0, 0, tiled=True)
 
 
-PIECE_STEPS = (0, 1, -1, -2, 2, 3, -3, -4)
+PIECE_STEPS = (0, 1, -1, -2, 2, 3, 4, -3)
 
 
 def layer_kernel(where_ref, sink_ref, x_ref, *refs):
     pieces = []
-    for first, second, third in (refs[:3], refs[3:6]):
+    for first, second, third, fourth in (refs[:4], refs[4:8]):
         pieces += [(first, k * 128) for k in range(4)]
-        pieces += [(second, k * 128) for k in range(3)] + [(third, 0)]
-    turn_ref, qg_ref, kg_ref, conv_ref, out_ref = refs[6:11]
-    w_s, p_s, kv_s, kk_s, vv_s, prod_s, act_s = refs[11:]
+        pieces += [(second, 0), (second, 128), (third, 0), (fourth, 0)]
+    turn_ref, qg_ref, kg_ref, conv_ref, out_ref = refs[8:13]
+    w_s, p_s, kv_s, kk_s, vv_s, prod_s, act_s = refs[13:]
     core, y, z, place = where_ref[0], where_ref[1], where_ref[2], where_ref[3]
 
     for k, (piece, base) in enumerate(pieces):

time: 116 us -> 117 us (level)
  the two profiles are of different devices: /device:TPU:17 before, /device:TPU:64 now
where the time goes in v4:
time: 117 us; the launch traced here: 116 us
  starting transfers between devices  42.6 us (36%)
  blocking collectives  41 us (35%)
  waiting for transfers between devices  16.7 us (14%)
  Pallas kernels  14.3 us (12%)
  other arithmetic  1.35 us (1%)
    all_to_all x1, blocking collectives, gathered_weights(): lax.all_to_all(blocks, 'sp', 0, 0, axis_index_groups=GROUPS, tiled=True)  20.7 us
    all_to_all x1, blocking collectives, per_device(): lax.all_to_all(partial.reshape(TP, LOCAL, -1), 'tp', 0, 0, tiled=True)  20.2 us
    ppermute x4, starting transfers between devices, gathered_weights(): return kept + tuple((lax.ppermute(p, 'sp', SWAP) for p in kept))  8.15 us
    ppermute x1, waiting for transfers between devices, gathered_weights(): o3 = lax.ppermute(e2, 'sp', ODD)  7.73 us
    all_to_all x1, starting transfers between devices, gathered_tokens(): return lax.all_to_all(sent, 'tp', 0, 0, tiled=True)  7.05 us
    pallas_call x1, Pallas kernels, run_layer(): pl.pallas_call(layer_kernel, out_shape=jax.ShapeDtypeStruct((MAIN, featur...  6.98 us
    ppermute x1, starting transfers between devices, gathered_weights(): o2 = lax.ppermute(e1, 'sp', ODD)  5.47 us
    ppermute x1, starting transfers between devices, gathered_weights(): o1 = lax.ppermute(own, 'sp', ODD)  5.15 us
  transfers between devices with their start and end apart: 13, of which 5 were waited for; matrix products, arithmetic and copies ran while one was open for 0% of the time, Pallas kernels for 5%

profile of v4, /device:TPU:64, one launch (start us, length us, event | category | flops | bytes accessed | tf_op | source)
XLA Modules:
  0.0 116.2 jit_solution(4331047502676864247)
XLA Ops:
  0.0 1.7 %copies.1 = bf16[8,16,1664]{2,1,0:T(8,128)(2,1)} custom-call(bf16[16,256]{1,0:T(8,128)(2,1)} %bitcast.23, bf16[16,64]{1,0:T(8,128)(2,1)} %bitcast.30, bf16[16,64]{1,0:T(8,128)(2,1)} %bitcast.31, bf16[16,256]{1,0:T(8,128)(2,1)} %bitcast.24, bf16[16,256]{1,0:T(8,128)(2,1)} %bitcast.25, bf16[16,256]{1,0:T(8,128)(2,1)} %bitcast.26, bf16[16,256]{1,0:T(8,128)(2,1)} %bitcast.27, ...), custom_call_target="tpu_custom_call" | custom-call | tf_op jit(solution)/shard_map/copies/pallas_call | solution.py:81
  1.7 20.7 %all_to_all.15 = bf16[8,16,1664]{2,1,0:T(8,128)(2,1)S(1)} all-to-all(bf16[8,16,1664]{2,1,0:T(8,128)(2,1)} %copies.1), channel_id=1, replica_groups={{0,64,128,192,256,320,384,448},{8,72,136,200,264,328,392,456},{16,80,14..., dimensions={0} | all-to-all | bytes 851968 | tf_op jit(solution)/shard_map/all_to_all | solution.py:109
  22.4 3.5 %collective-permute-start.1 = (bf16[128,1664]{1,0:T(8,128)(2,1)S(1)}, bf16[128,1664]{1,0:T(8,128)(2,1)S(1)}, u32[]{:S(2)}, u32[]{:S(2)}) collective-permute-start(bf16[128,1664]{1,0:T(8,128)(2,1)S(1)} %bitcast.18), channel_id=1, source_target_pairs={{0,8},{4,68},{8,0},{12,76},{16,24},{20,84},{24,16},{28,92},{32,40}... | collective-permute-start | bytes 1277960 | tf_op jit(solution)/shard_map/ppermute | solution.py:111
  25.9 5.1 %collective-permute-start.2 = (bf16[128,1664]{1,0:T(8,128)(2,1)S(1)}, bf16[128,1664]{1,0:T(8,128)(2,1)S(1)}, u32[]{:S(2)}, u32[]{:S(2)}) collective-permute-start(bf16[128,1664]{1,0:T(8,128)(2,1)S(1)} %bitcast.19), channel_id=1, source_target_pairs={{0,56},{4,452},{8,16},{12,460},{16,8},{20,468},{24,32},{28,476},{3... | collective-permute-start | bytes 1277960 | tf_op jit(solution)/shard_map/ppermute | solution.py:112
  31.0 1.4 %collective-permute-done.1.refs_1_ = bf16[128,1664]{1,0:T(8,128)(2,1)S(1)} collective-permute-done((bf16[128,1664]{1,0:T(8,128)(2,1)S(1)}, bf16[128,1664]{1,0:T(8,128)(2,1)S(1)}, u32[]{:S(2)}, u32[]{:S(2)}) %collective-permute-start.1) | collective-permute-done | bytes 426016 | tf_op jit(solution)/shard_map/ppermute | solution.py:111
  32.4 5.5 %collective-permute-start.3 = (bf16[128,1664]{1,0:T(8,128)(2,1)S(1)}, bf16[128,1664]{1,0:T(8,128)(2,1)S(1)}, u32[]{:S(2)}, u32[]{:S(2)}) collective-permute-start(bf16[128,1664]{1,0:T(8,128)(2,1)S(1)} %collective-permute-done.1.refs_1_), channel_id=1, source_target_pairs={{0,56},{4,452},{8,16},{12,460},{16,8},{20,468},{24,32},{28,476},{3... | collective-permute-start | bytes 1277960 | tf_op jit(solution)/shard_map/ppermute | solution.py:113
  37.9 1.8 %norm.1.normed = bf16[64,2048]{1,0:T(8,128)(2,1)} custom-call(bf16[64,2048]{1,0:T(8,128)(2,1)} %x_ref.1, f32[1,2048]{1,0:T(1,128)} %bitcast.29), custom_call_target="tpu_custom_call" | custom-call | tf_op jit(solution)/shard_map/norm/pallas_call | solution.py:146
  39.7 2.0 %collective-permute-start = (bf16[64,2048]{1,0:T(8,128)(2,1)}, bf16[64,2048]{1,0:T(8,128)(2,1)S(1)}, u32[]{:S(2)}, u32[]{:S(2)}) collective-permute-start(bf16[64,2048]{1,0:T(8,128)(2,1)} %norm.1.normed), channel_id=1, source_target_pairs={{2,6},{3,7},{6,10},{7,11},{10,14},{11,15},{14,18},{15,19},{18,22},... | collective-permute-start | bytes 786440 | tf_op jit(solution)/shard_map/ppermute | solution.py:156
  41.8 2.2 %collective-permute-done.3.refs_3_ = bf16[128,1664]{1,0:T(8,128)(2,1)S(1)} collective-permute-done((bf16[128,1664]{1,0:T(8,128)(2,1)S(1)}, bf16[128,1664]{1,0:T(8,128)(2,1)S(1)}, u32[]{:S(2)}, u32[]{:S(2)}) %collective-permute-start.3) | collective-permute-done | bytes 426016 | tf_op jit(solution)/shard_map/ppermute | solution.py:113
  44.0 1.3 %shard_map.145.refs_0_ = bf16[512,1664]{1,0:T(8,128)(2,1)} custom-call(bf16[128,1664]{1,0:T(8,128)(2,1)S(1)} %bitcast.20, bf16[128,1664]{1,0:T(8,128)(2,1)S(1)} %collective-permute-done.1.refs_1_, bf16[128,1664]{1,0:T(8,128)(2,1)S(1)} %collective-permute-done.2.refs_2_, bf16[128,1664]{1,0:T(8,128)(2,1)S(1)} %collective-permute-done.3.refs_3_), custom_call_target="tpu_custom_call" | custom-call | tf_op jit(solution)/shard_map/pallas_call | solution.py:130
  45.3 1.9 %collective-permute-start.8 = (bf16[512,1664]{1,0:T(8,128)(2,1)}, bf16[512,1664]{1,0:T(8,128)(2,1)}, u32[]{:S(2)}, u32[]{:S(2)}) collective-permute-start(bf16[512,1664]{1,0:T(8,128)(2,1)} %shard_map.145.refs_0_), channel_id=1, source_target_pairs={{0,4},{4,0},{8,12},{12,8},{16,20},{20,16},{24,28},{28,24},{32,36},... | collective-permute-start | bytes 5111816 | tf_op jit(solution)/shard_map/ppermute | solution.py:121
  47.2 1.5 %rows.1 = bf16[4,128,2048]{2,1,0:T(8,128)(2,1)} custom-call(bf16[64,2048]{1,0:T(8,128)(2,1)S(1)} %copy-done, bf16[64,2048]{1,0:T(8,128)(2,1)S(1)} %collective-permute-done.rim), custom_call_target="tpu_custom_call" | custom-call | tf_op jit(solution)/shard_map/rows/pallas_call | solution.py:97
  48.7 7.1 %all-to-all-start = ((bf16[4,128,2048]{2,1,0:T(8,128)(2,1)}), bf16[4,128,2048]{2,1,0:T(8,128)(2,1)S(1)}, u32[]{:S(2)}, u32[]{:S(2)}) async-start(bf16[4,128,2048]{2,1,0:T(8,128)(2,1)} %rows.1), calls=%async_computation | async-start | bytes 4194304 | tf_op jit(solution)/shard_map/all_to_all | solution.py:158
  55.8 2.1 %collective-permute-start.4 = (bf16[128,1664]{1,0:T(8,128)(2,1)S(1)}, bf16[128,1664]{1,0:T(8,128)(2,1)}, u32[]{:S(2)}, u32[]{:S(2)}) collective-permute-start(bf16[128,1664]{1,0:T(8,128)(2,1)S(1)} %collective-permute-done.2.refs_2_), channel_id=1, source_target_pairs={{0,8},{4,68},{8,0},{12,76},{16,24},{20,84},{24,16},{28,92},{32,40}... | collective-permute-start | bytes 1277960 | tf_op jit(solution)/shard_map/ppermute | solution.py:114
  57.8 3.9 %collective-permute-start.5 = (bf16[128,1664]{1,0:T(8,128)(2,1)S(1)}, bf16[128,1664]{1,0:T(8,128)(2,1)S(1)}, u32[]{:S(2)}, u32[]{:S(2)}) collective-permute-start(bf16[128,1664]{1,0:T(8,128)(2,1)S(1)} %collective-permute-done.3.refs_3_), channel_id=1, source_target_pairs={{0,8},{4,68},{8,0},{12,76},{16,24},{20,84},{24,16},{28,92},{32,40}... | collective-permute-start | bytes 1277960 | tf_op jit(solution)/shard_map/ppermute | solution.py:115
  61.8 4.3 %collective-permute-done.4.refs_0_ = bf16[128,1664]{1,0:T(8,128)(2,1)} collective-permute-done((bf16[128,1664]{1,0:T(8,128)(2,1)S(1)}, bf16[128,1664]{1,0:T(8,128)(2,1)}, u32[]{:S(2)}, u32[]{:S(2)}) %collective-permute-start.4) | collective-permute-done | bytes 426016 | tf_op jit(solution)/shard_map/ppermute | solution.py:114
  66.0 2.5 %collective-permute-start.7 = (bf16[128,1664]{1,0:T(8,128)(2,1)}, bf16[128,1664]{1,0:T(8,128)(2,1)}, u32[]{:S(2)}, u32[]{:S(2)}) collective-permute-start(bf16[128,1664]{1,0:T(8,128)(2,1)} %collective-permute-done.4.refs_0_), channel_id=1, source_target_pairs={{0,56},{4,452},{8,16},{12,460},{16,8},{20,468},{24,32},{28,476},{3... | collective-permute-start | bytes 1277960 | tf_op jit(solution)/shard_map/ppermute | solution.py:116
  68.5 2.8 %collective-permute-start.6 = (bf16[128,1664]{1,0:T(8,128)(2,1)S(1)}, bf16[128,1664]{1,0:T(8,128)(2,1)}, u32[]{:S(2)}, u32[]{:S(2)}) collective-permute-start(bf16[128,1664]{1,0:T(8,128)(2,1)S(1)} %collective-permute-done.3.refs_3_), channel_id=1, source_target_pairs={{0,16},{4,132},{8,56},{12,140},{16,32},{20,148},{24,8},{28,156},{3... | collective-permute-start | bytes 1277960 | tf_op jit(solution)/shard_map/ppermute | solution.py:117
  72.4 1.9 %collective-permute-start.9 = (bf16[256,1664]{1,0:T(8,128)(2,1)S(1)}, bf16[256,1664]{1,0:T(8,128)(2,1)}, u32[]{:S(2)}, u32[]{:S(2)}) collective-permute-start(bf16[256,1664]{1,0:T(8,128)(2,1)S(1)} %shard_map.146.refs_1_), channel_id=1, source_target_pairs={{0,4},{4,0},{8,12},{12,8},{16,20},{20,16},{24,28},{28,24},{32,36},... | collective-permute-start | bytes 2555912 | tf_op jit(solution)/shard_map/ppermute | solution.py:121
  74.4 7.7 %collective-permute-done.7.refs_3_ = bf16[128,1664]{1,0:T(8,128)(2,1)} collective-permute-done((bf16[128,1664]{1,0:T(8,128)(2,1)}, bf16[128,1664]{1,0:T(8,128)(2,1)}, u32[]{:S(2)}, u32[]{:S(2)}) %collective-permute-start.7) | collective-permute-done | bytes 426016 | tf_op jit(solution)/shard_map/ppermute | solution.py:116
  82.1 1.9 %collective-permute-start.11 = (bf16[128,1664]{1,0:T(8,128)(2,1)}, bf16[128,1664]{1,0:T(8,128)(2,1)}, u32[]{:S(2)}, u32[]{:S(2)}) collective-permute-start(bf16[128,1664]{1,0:T(8,128)(2,1)} %collective-permute-done.7.refs_3_), channel_id=1, source_target_pairs={{0,4},{4,0},{8,12},{12,8},{16,20},{20,16},{24,28},{28,24},{32,36},... | collective-permute-start | bytes 1277960 | tf_op jit(solution)/shard_map/ppermute | solution.py:121
  84.1 2.4 %collective-permute-start.10 = (bf16[128,1664]{1,0:T(8,128)(2,1)}, bf16[128,1664]{1,0:T(8,128)(2,1)S(1)}, u32[]{:S(2)}, u32[]{:S(2)}) collective-permute-start(bf16[128,1664]{1,0:T(8,128)(2,1)} %collective-permute-done.6.refs_2_), channel_id=1, source_target_pairs={{0,4},{4,0},{8,12},{12,8},{16,20},{20,16},{24,28},{28,24},{32,36},... | collective-permute-start | bytes 1277960 | tf_op jit(solution)/shard_map/ppermute | solution.py:121
  88.1 7.0 %layer.1 = bf16[256,2048]{1,0:T(8,128)(2,1)S(1)} custom-call(s32[4]{0:T(128)S(1)} %pad_add_fusion.where_ref, f32[4]{0:T(128)S(1)} %copy-done.2, bf16[4,128,2048]{2,1,0:T(8,128)(2,1)S(1)} %all-to-all-done.x_ref, bf16[512,1664]{1,0:T(8,128)(2,1)} %shard_map.145.refs_0_, bf16[256,1664]{1,0:T(8,128)(2,1)S(1)} %shard_map.146.refs_1_, ...), custom_call_target="tpu_custom_call" | custom-call | tf_op jit(solution)/shard_map/layer/pallas_call | solution.py:299
  95.1 20.2 %all_to_all.16 = bf16[4,64,2048]{2,1,0:T(8,128)(2,1)S(1)} all-to-all(bf16[4,64,2048]{2,1,0:T(8,128)(2,1)S(1)} %bitcast.17), channel_id=1, replica_groups=mesh['sp'=128,'tp'=4] {'tp'}, dimensions={0} | all-to-all | bytes 2097152 | tf_op jit(solution)/shard_map/all_to_all | solution.py:355
  (29 shorter events, 3.6 us)
Async XLA Ops:
  22.4 10.0 %collective-permute-start.1 = (bf16[128,1664]{1,0:T(8,128)(2,1)S(1)}, bf16[128,1664]{1,0:T(8,128)(2,1)S(1)}, u32[]{:S(2)}, u32[]{:S(2)}) collective-permute-start(bf16[128,1664]{1,0:T(8,128)(2,1)S(1)} %bitcast.18), channel_id=1, source_target_pairs={{0,8},{4,68},{8,0},{12,76},{16,24},{20,84},{24,16},{28,92},{32,40}... | collective-permute-start | bytes 1277960 | tf_op jit(solution)/shard_map/ppermute | solution.py:111
  25.9 15.9 %collective-permute-start.2 = (bf16[128,1664]{1,0:T(8,128)(2,1)S(1)}, bf16[128,1664]{1,0:T(8,128)(2,1)S(1)}, u32[]{:S(2)}, u32[]{:S(2)}) collective-permute-start(bf16[128,1664]{1,0:T(8,128)(2,1)S(1)} %bitcast.19), channel_id=1, source_target_pairs={{0,56},{4,452},{8,16},{12,460},{16,8},{20,468},{24,32},{28,476},{3... | collective-permute-start | bytes 1277960 | tf_op jit(solution)/shard_map/ppermute | solution.py:112
  32.4 11.6 %collective-permute-start.3 = (bf16[128,1664]{1,0:T(8,128)(2,1)S(1)}, bf16[128,1664]{1,0:T(8,128)(2,1)S(1)}, u32[]{:S(2)}, u32[]{:S(2)}) collective-permute-start(bf16[128,1664]{1,0:T(8,128)(2,1)S(1)} %collective-permute-done.1.refs_1_), channel_id=1, source_target_pairs={{0,56},{4,452},{8,16},{12,460},{16,8},{20,468},{24,32},{28,476},{3... | collective-permute-start | bytes 1277960 | tf_op jit(solution)/shard_map/ppermute | solution.py:113
  39.7 7.5 %copy-start = (bf16[64,2048]{1,0:T(8,128)(2,1)S(1)}, bf16[64,2048]{1,0:T(8,128)(2,1)}, u32[]{:S(2)}) copy-start(bf16[64,2048]{1,0:T(8,128)(2,1)} %norm.1.normed) | copy-start | bytes 786436
  39.7 7.5 %collective-permute-start = (bf16[64,2048]{1,0:T(8,128)(2,1)}, bf16[64,2048]{1,0:T(8,128)(2,1)S(1)}, u32[]{:S(2)}, u32[]{:S(2)}) collective-permute-start(bf16[64,2048]{1,0:T(8,128)(2,1)} %norm.1.normed), channel_id=1, source_target_pairs={{2,6},{3,7},{6,10},{7,11},{10,14},{11,15},{14,18},{15,19},{18,22},... | collective-permute-start | bytes 786440 | tf_op jit(solution)/shard_map/ppermute | solution.py:156
  45.3 42.8 %collective-permute-start.8 = (bf16[512,1664]{1,0:T(8,128)(2,1)}, bf16[512,1664]{1,0:T(8,128)(2,1)}, u32[]{:S(2)}, u32[]{:S(2)}) collective-permute-start(bf16[512,1664]{1,0:T(8,128)(2,1)} %shard_map.145.refs_0_), channel_id=1, source_target_pairs={{0,4},{4,0},{8,12},{12,8},{16,20},{20,16},{24,28},{28,24},{32,36},... | collective-permute-start | bytes 5111816 | tf_op jit(solution)/shard_map/ppermute | solution.py:121
  48.7 37.9 %copy-start.5 = (f32[128]{0:T(128)S(1)}, f32[128]{0:T(128)}, u32[]{:S(2)}) copy-start(f32[128]{0:T(128)} %constant.47.clone) | copy-start | bytes 1540
  48.7 38.2 %all-to-all-start = ((bf16[4,128,2048]{2,1,0:T(8,128)(2,1)}), bf16[4,128,2048]{2,1,0:T(8,128)(2,1)S(1)}, u32[]{:S(2)}, u32[]{:S(2)}) async-start(bf16[4,128,2048]{2,1,0:T(8,128)(2,1)} %rows.1), calls=%async_computation | async-start | bytes 4194304 | tf_op jit(solution)/shard_map/all_to_all | solution.py:158
  55.8 32.3 %copy-start.1 = (f32[3,256]{1,0:T(4,128)S(1)}, f32[3,256]{1,0:T(4,128)}, u32[]{:S(2)}) copy-start(f32[3,256]{1,0:T(4,128)} %refs_11_.1) | copy-start | bytes 9220
  55.8 32.3 %copy-start.2 = (f32[4]{0:T(128)S(1)}, f32[4]{0:T(128)}, u32[]{:S(2)}) copy-start(f32[4]{0:T(128)} %sink_ref.1) | copy-start | bytes 52
  55.8 32.3 %copy-start.3 = (f32[64]{0:T(128)S(1)}, f32[64]{0:T(128)}, u32[]{:S(2)}) copy-start(f32[64]{0:T(128)} %param.23) | copy-start | bytes 772
  55.8 32.3 %copy-start.4 = (f32[64]{0:T(128)S(1)}, f32[64]{0:T(128)}, u32[]{:S(2)}) copy-start(f32[64]{0:T(128)} %param.24) | copy-start | bytes 772
  55.8 10.3 %collective-permute-start.4 = (bf16[128,1664]{1,0:T(8,128)(2,1)S(1)}, bf16[128,1664]{1,0:T(8,128)(2,1)}, u32[]{:S(2)}, u32[]{:S(2)}) collective-permute-start(bf16[128,1664]{1,0:T(8,128)(2,1)S(1)} %collective-permute-done.2.refs_2_), channel_id=1, source_target_pairs={{0,8},{4,68},{8,0},{12,76},{16,24},{20,84},{24,16},{28,92},{32,40}... | collective-permute-start | bytes 1277960 | tf_op jit(solution)/shard_map/ppermute | solution.py:114
  57.8 13.5 %collective-permute-start.5 = (bf16[128,1664]{1,0:T(8,128)(2,1)S(1)}, bf16[128,1664]{1,0:T(8,128)(2,1)S(1)}, u32[]{:S(2)}, u32[]{:S(2)}) collective-permute-start(bf16[128,1664]{1,0:T(8,128)(2,1)S(1)} %collective-permute-done.3.refs_3_), channel_id=1, source_target_pairs={{0,8},{4,68},{8,0},{12,76},{16,24},{20,84},{24,16},{28,92},{32,40}... | collective-permute-start | bytes 1277960 | tf_op jit(solution)/shard_map/ppermute | solution.py:115
  66.0 16.1 %collective-permute-start.7 = (bf16[128,1664]{1,0:T(8,128)(2,1)}, bf16[128,1664]{1,0:T(8,128)(2,1)}, u32[]{:S(2)}, u32[]{:S(2)}) collective-permute-start(bf16[128,1664]{1,0:T(8,128)(2,1)} %collective-permute-done.4.refs_0_), channel_id=1, source_target_pairs={{0,56},{4,452},{8,16},{12,460},{16,8},{20,468},{24,32},{28,476},{3... | collective-permute-start | bytes 1277960 | tf_op jit(solution)/shard_map/ppermute | solution.py:116
  68.5 15.5 %collective-permute-start.6 = (bf16[128,1664]{1,0:T(8,128)(2,1)S(1)}, bf16[128,1664]{1,0:T(8,128)(2,1)}, u32[]{:S(2)}, u32[]{:S(2)}) collective-permute-start(bf16[128,1664]{1,0:T(8,128)(2,1)S(1)} %collective-permute-done.3.refs_3_), channel_id=1, source_target_pairs={{0,16},{4,132},{8,56},{12,140},{16,32},{20,148},{24,8},{28,156},{3... | collective-permute-start | bytes 1277960 | tf_op jit(solution)/shard_map/ppermute | solution.py:117
  72.4 15.7 %collective-permute-start.9 = (bf16[256,1664]{1,0:T(8,128)(2,1)S(1)}, bf16[256,1664]{1,0:T(8,128)(2,1)}, u32[]{:S(2)}, u32[]{:S(2)}) collective-permute-start(bf16[256,1664]{1,0:T(8,128)(2,1)S(1)} %shard_map.146.refs_1_), channel_id=1, source_target_pairs={{0,4},{4,0},{8,12},{12,8},{16,20},{20,16},{24,28},{28,24},{32,36},... | collective-permute-start | bytes 2555912 | tf_op jit(solution)/shard_map/ppermute | solution.py:121
  82.1 4.8 %collective-permute-start.11 = (bf16[128,1664]{1,0:T(8,128)(2,1)}, bf16[128,1664]{1,0:T(8,128)(2,1)}, u32[]{:S(2)}, u32[]{:S(2)}) collective-permute-start(bf16[128,1664]{1,0:T(8,128)(2,1)} %collective-permute-done.7.refs_3_), channel_id=1, source_target_pairs={{0,4},{4,0},{8,12},{12,8},{16,20},{20,16},{24,28},{28,24},{32,36},... | collective-permute-start | bytes 1277960 | tf_op jit(solution)/shard_map/ppermute | solution.py:121
  84.1 4.0 %collective-permute-start.10 = (bf16[128,1664]{1,0:T(8,128)(2,1)}, bf16[128,1664]{1,0:T(8,128)(2,1)S(1)}, u32[]{:S(2)}, u32[]{:S(2)}) collective-permute-start(bf16[128,1664]{1,0:T(8,128)(2,1)} %collective-permute-done.6.refs_2_), channel_id=1, source_target_pairs={{0,4},{4,0},{8,12},{12,8},{16,20},{20,16},{24,28},{28,24},{32,36},... | collective-permute-start | bytes 1277960 | tf_op jit(solution)/shard_map/ppermute | solution.py:121
